TPU v7x, 32 devices: a whole 2x2x4 slice. The times are simulated.
32 devices in a mesh: sp: 16 (over z, y, core), tp: 2 (over x).
Axes of the slice: x: 2, y: 2, z: 4, core: 2. Of those that a mesh axis runs over, the one named last changes fastest.
Arguments:
- queries: bfloat16 [16384, 1024], P('sp', 'tp'), may hold values from -8 to 8
- keyvals: bfloat16 [16384, 8, 128], P('sp', 'tp'), may hold values from -8 to 8
- head_sink_logit: float32 [16], P('tp'), may hold values from 2 to 7
- doc_ids: int32 [16384], P('sp'), may hold values from 0 to 7, never falling along the last dimension, each value on 1 to 4096 neighbouring positions
- stream_in: bfloat16 [16384, 2048], P(('sp', 'tp')), may hold values from -6 to 6
- out_weight: bfloat16 [1024, 2048], replicated, may hold values from -1.5 to 1.5
- first_gain: float32 [2048], replicated, may hold values from 0.1 to 1.9
- up_weight: bfloat16 [2048, 8192], P('sp', 'tp'), may hold values from -0.125 to 0.125
- down_weight: bfloat16 [8192, 2048], P('tp', 'sp'), may hold values from -0.0625 to 0.0625
- second_gain: float32 [2048], replicated, may hold values from 0.1 to 1.9
Outputs:
- layer_out: bfloat16 [16384, 2048], P(('sp', 'tp'))
Inputs may be any that keep to these rules, and one draw needn't show every extreme that they name: `doc_ids`: document numbers never fall along the sequence.
All inputs are finite; a program needn't handle non-finite values.
Results may differ from a plain program's by a relative error of at most 0.013.
Values may be sent and summed in bfloat16 or wider, within the bound.
No kernel may reach another device: no remote copies, remote signals or barrier semaphores. Data moves between devices by JAX's collectives and lax.ppermute only.
A program may use at most 128 MiB of HBM per device.

v0:
```python
import jax
import jax.numpy as jnp
from jax import lax
from jax.sharding import PartitionSpec as P

HEAD_SIZE = 64
WINDOW_REACH = 128


NEG_LARGE = -1e30
NORM_EPS = 1e-05


def padded(block, sides, width):
    for axis, dim in sides:
        count = lax.axis_size(axis)
        forward = [(i, i + 1) for i in range(count - 1)]
        backward = [(target, source) for source, target in forward]
        low = lax.ppermute(
            lax.slice_in_dim(block, block.shape[dim] - width, None, axis=dim), axis, forward
        )
        high = lax.ppermute(lax.slice_in_dim(block, 0, width, axis=dim), axis, backward)
        block = jnp.concatenate([low, block, high], axis=dim)
    return block


def layer_norm(stream, gain_row):
    centre = jnp.mean(stream, axis=-1, keepdims=True)
    shifted = stream - centre
    spread = jnp.mean(shifted * shifted, axis=-1, keepdims=True)
    return shifted * lax.rsqrt(spread + NORM_EPS) * gain_row


def attend(queries, keyvals, head_sink_logit, doc_ids):
    tok_rows = queries.shape[0]
    kv_heads = keyvals.shape[1]
    heads_per_group = queries.shape[1] // (HEAD_SIZE * kv_heads)
    block_list = tok_rows // WINDOW_REACH
    score_scale = HEAD_SIZE ** (-0.5)
    doc_marks = doc_ids.astype(jnp.bfloat16)
    rim_keys, rim_docs = (
        padded(keyvals, (("sp", 0),), WINDOW_REACH),
        padded(doc_marks, (("sp", 0),), WINDOW_REACH),
    )
    padded_rows = rim_keys.reshape(block_list + 2, WINDOW_REACH, kv_heads, 2 * HEAD_SIZE)
    banded = jnp.concatenate([padded_rows[:-2], padded_rows[1:-1], padded_rows[2:]], axis=1)
    doc_ext = rim_docs.reshape(block_list + 2, WINDOW_REACH)
    doc_band = jnp.concatenate([doc_ext[:-2], doc_ext[1:-1], doc_ext[2:]], axis=1)
    offset = lax.axis_index("sp") * tok_rows
    total_rows = tok_rows * lax.axis_size("sp")
    query_pos = offset + jnp.arange(tok_rows, dtype=jnp.int32).reshape(block_list, WINDOW_REACH, 1)
    key_pos = (
        offset
        + (
            jnp.arange(block_list, dtype=jnp.int32)[:, None] * WINDOW_REACH
            + jnp.arange(3 * WINDOW_REACH, dtype=jnp.int32)[None, :]
            - WINDOW_REACH
        )[:, None, :]
    )
    allowed = (
        (jnp.abs(query_pos - key_pos) <= WINDOW_REACH)
        & (key_pos >= 0)
        & (key_pos < total_rows)
        & (doc_marks.reshape(block_list, WINDOW_REACH, 1) == doc_band[:, None, :])
    )
    query_block_list = queries.reshape(
        block_list, WINDOW_REACH, kv_heads, heads_per_group, HEAD_SIZE
    )
    scores = (
        jnp.einsum(
            "nqhgd,nkhd->nhgqk",
            query_block_list,
            banded[..., :HEAD_SIZE],
            preferred_element_type=jnp.float32,
        )
        * score_scale
    )
    scores = jnp.where(allowed[:, None, None], scores, NEG_LARGE)
    sink_col = head_sink_logit.reshape(kv_heads, heads_per_group)[None, :, :, None, None]
    highest = jnp.maximum(jnp.max(scores, axis=-1, keepdims=True), sink_col)
    powers = jnp.exp(scores - highest)
    denominator = jnp.sum(powers, axis=-1, keepdims=True) + jnp.exp(sink_col - highest)
    weights = (powers / denominator).astype(jnp.bfloat16)
    mixed_out = jnp.einsum(
        "nhgqk,nkhd->nqhgd", weights, banded[..., HEAD_SIZE:], preferred_element_type=jnp.float32
    )
    return mixed_out.astype(jnp.bfloat16).reshape(tok_rows, kv_heads * heads_per_group * HEAD_SIZE)


def per_device(
    queries,
    keyvals,
    head_sink_logit,
    doc_ids,
    stream_in,
    out_weight,
    first_gain,
    up_weight,
    down_weight,
    second_gain,
):
    up_whole = lax.all_gather(up_weight, "sp", axis=0, tiled=True)
    down_whole = lax.all_gather(down_weight, "sp", axis=1, tiled=True)
    attended = attend(queries, keyvals, head_sink_logit, doc_ids)
    tp_count = lax.axis_size("tp")
    own_rows = attended.shape[0] // tp_count
    by_peer = attended.reshape(tp_count, own_rows, attended.shape[1])
    projected = jnp.dot(
        lax.all_to_all(by_peer, "tp", split_axis=0, concat_axis=2, tiled=True)[0],
        out_weight,
        preferred_element_type=jnp.float32,
    )[None][0]
    first_stream = layer_norm(stream_in.astype(jnp.float32) + projected, first_gain).astype(
        jnp.bfloat16
    )
    hidden = jnp.dot(
        lax.all_gather(first_stream, "tp", axis=0, tiled=True),
        up_whole,
        preferred_element_type=jnp.float32,
    )
    active = jnp.square(jnp.maximum(hidden, 0.0)).astype(jnp.bfloat16)
    mixed_out = lax.psum_scatter(
        jnp.dot(active, down_whole, preferred_element_type=jnp.float32).astype(jnp.bfloat16),
        "tp",
        scatter_dimension=0,
        tiled=True,
    ).astype(jnp.float32)
    return layer_norm(first_stream.astype(jnp.float32) + mixed_out, second_gain).astype(
        jnp.bfloat16
    )


def solution(mesh):
    return jax.shard_map(
        per_device,
        mesh=mesh,
        in_specs=(
            P("sp", "tp"),
            P("sp", "tp", None),
            P("tp"),
            P("sp"),
            P(("sp", "tp"), None),
            P(),
            P(),
            P("sp", "tp"),
            P("tp", "sp"),
            P(),
        ),
        out_specs=P(("sp", "tp"), None),
        check_vma=False,
    )
```

profile of v0, /device:TPU:0, one launch (start us, length us, event | category | flops | bytes accessed | tf_op | source)
XLA Modules:
  0.0 477.8 jit_solution(12057201046544516895)
XLA Ops:
  7.3 2.4 collective-permute-start.2
  9.7 1.3 collective-permute-start.3
  11.0 1.4 copy.26
  12.4 5.8 %collective-permute-start = (bf16[128,4,128]{2,0,1:T(8,128)(2,1)S(1)}, bf16[128,4,128]{2,0,1:T(8,128)(2,1)}, u32[]{:S(2)}, u32[]{:S(2)}) collective-permute-start(bf16[128,4,128]{2,0,1:T(8,128)(2,1)S(1)} %get-tuple-element.7), channel_id=1, source_target_pairs={{0,2},{2,4},{4,6},{6,8},{8,10},{10,12},{12,14},{14,16},{16,18},{18... | collective-permute-start | bytes 393224 | tf_op jit(solution)/shard_map/ppermute | solution.py:19
  18.2 1.3 collective-permute-start.1
  20.4 2.3 copy.32
  22.6 2.1 reshape.167
  24.8 2.3 fusion.9
  29.7 1.8 pad_maximum_fusion
  31.6 2.5 fusion.1
  34.3 3.4 fusion
  37.8 3.6 fusion.11
  42.8 17.2 %all_to_all.15 = bf16[2,512,512]{1,2,0:T(8,128)(2,1)S(1)} all-to-all(bf16[2,512,512]{1,2,0:T(8,128)(2,1)S(1)} %copy.38), channel_id=1, replica_groups=mesh['sp'=16,'tp'=2] {'tp'}, dimensions={0} | all-to-all | bytes 2097152 | tf_op jit(solution)/shard_map/all_to_all | solution.py:109
  60.0 4.2 fusion.20
  64.8 1.4 copy-done
  66.1 1.9 multiply_convert_fusion.2
  69.6 56.9 %all-gather.4.cloned.1.call-done = bf16[1024,2048]{1,0:T(8,128)(2,1)} async-done(((bf16[512,2048]{1,0:T(8,128)(2,1)}), bf16[1024,2048]{1,0:T(8,128)(2,1)}) %all-gather.4.cloned.1.call-update) | async-done | bytes 4194320 | tf_op jit(solution)/shard_map/all_gather | solution.py:117
  126.5 128.6 %all-gather.6.cloned.1.call-done = bf16[2048,4096]{1,0:T(8,128)(2,1)} async-done(((bf16[128,4096]{1,0:T(8,128)(2,1)}), bf16[2048,4096]{1,0:T(8,128)(2,1)}) %all-gather.6.cloned.1.call-update) | async-done | bytes 16777232 | tf_op jit(solution)/shard_map/all_gather | solution.py:102
  255.1 22.9 %fusion.44 = bf16[1024,4096]{1,0:T(8,128)(2,1)} fusion(bf16[2048,4096]{1,0:T(8,128)(2,1)} %all-gather.6.cloned.1.call-done, bf16[1024,2048]{1,0:T(8,128)(2,1)} %all-gather.4.cloned.1.call-done), kind=kOutput, calls=%bitcast_fusion.1.clone.1 | convolution fusion | flops 17192452096 | bytes 29360128 | tf_op jit(solution)/shard_map/dot_general | solution.py:116
  278.0 107.4 %all-gather.8.cloned.1.call-done = bf16[4096,2048]{1,0:T(8,128)(2,1)} async-done(((bf16[4096,128]{1,0:T(8,128)(2,1)}), bf16[4096,2048]{1,0:T(8,128)(2,1)}) %all-gather.8.cloned.1.call-update) | async-done | bytes 16777232 | tf_op jit(solution)/shard_map/all_gather | solution.py:103
  385.4 23.7 %convolution_convert_fusion = bf16[1024,2048]{1,0:T(8,128)(2,1)} fusion(bf16[4096,2048]{1,0:T(8,128)(2,1)} %all-gather.8.cloned.1.call-done, bf16[1024,4096]{1,0:T(8,128)(2,1)} %fusion.44), kind=kOutput, calls=%fused_computation.15 | convolution fusion | flops 17181966336 | bytes 29360128 | tf_op jit(solution)/shard_map/dot_general | solution.py:123
  409.1 52.7 %reduce-scatter.2.cloned.1.call-done = bf16[512,2048]{1,0:T(8,128)(2,1)} async-done(((bf16[1024,2048]{1,0:T(8,128)(2,1)}), bf16[512,2048]{1,0:T(8,128)(2,1)}) %reduce-scatter.2.cloned.1.call-update) | async-done | bytes 2097168 | tf_op jit(solution)/shard_map/reduce_scatter | solution.py:122
  461.8 3.9 fusion.4
  467.8 3.5 multiply_convert_fusion.1
  (58 shorter events, 10.0 us)
Async XLA Ops:
  6.5 16.1 %copy-start.7 = (bf16[1024,512]{1,0:T(8,128)(2,1)S(1)}, bf16[1024,512]{1,0:T(8,128)(2,1)}, u32[]{:S(2)}) copy-start(bf16[1024,512]{1,0:T(8,128)(2,1)} %param.10) | copy-start | bytes 3145732
  6.5 18.2 %copy-start.10 = (f32[8]{0:T(128)S(1)}, f32[8]{0:T(128)}, u32[]{:S(2)}) copy-start(f32[8]{0:T(128)} %param.12) | copy-start | bytes 100
  6.5 119.9 %all-gather.4.cloned.1.call-start = ((), (), s32[]{:S(2)}) async-start(), calls=%async_computation.2 | async-start | bytes 6291456 | tf_op jit(solution)/shard_map/all_gather | solution.py:117
  7.3 17.5 %collective-permute-start.2 = (bf16[128]{0:T(256)(128)(2,1)S(1)}, bf16[128]{0:T(256)(128)(2,1)S(1)}, u32[]{:S(2)}, u32[]{:S(2)}) collective-permute-start(bf16[128]{0:T(256)(128)(2,1)S(1)} %get-tuple-element.11), channel_id=1, source_target_pairs={{0,2},{2,4},{4,6},{6,8},{8,10},{10,12},{12,14},{14,16},{16,18},{18... | collective-permute-start | bytes 776 | tf_op jit(solution)/shard_map/ppermute | solution.py:19
  9.7 15.1 %collective-permute-start.3 = (bf16[128]{0:T(256)(128)(2,1)S(1)}, bf16[128]{0:T(256)(128)(2,1)S(1)}, u32[]{:S(2)}, u32[]{:S(2)}) collective-permute-start(bf16[128]{0:T(256)(128)(2,1)S(1)} %get-tuple-element.12), channel_id=1, source_target_pairs={{2,0},{4,2},{6,4},{8,6},{10,8},{12,10},{14,12},{16,14},{18,16},{20... | collective-permute-start | bytes 776 | tf_op jit(solution)/shard_map/ppermute | solution.py:22
  12.4 14.7 %collective-permute-start = (bf16[128,4,128]{2,0,1:T(8,128)(2,1)S(1)}, bf16[128,4,128]{2,0,1:T(8,128)(2,1)}, u32[]{:S(2)}, u32[]{:S(2)}) collective-permute-start(bf16[128,4,128]{2,0,1:T(8,128)(2,1)S(1)} %get-tuple-element.7), channel_id=1, source_target_pairs={{0,2},{2,4},{4,6},{6,8},{8,10},{10,12},{12,14},{14,16},{16,18},{18... | collective-permute-start | bytes 393224 | tf_op jit(solution)/shard_map/ppermute | solution.py:19
  18.2 8.9 %collective-permute-start.1 = (bf16[128,4,128]{2,0,1:T(8,128)(2,1)S(1)}, bf16[128,4,128]{2,0,1:T(8,128)(2,1)}, u32[]{:S(2)}, u32[]{:S(2)}) collective-permute-start(bf16[128,4,128]{2,0,1:T(8,128)(2,1)S(1)} %get-tuple-element.8), channel_id=1, source_target_pairs={{2,0},{4,2},{6,4},{8,6},{10,8},{12,10},{14,12},{16,14},{18,16},{20... | collective-permute-start | bytes 393224 | tf_op jit(solution)/shard_map/ppermute | solution.py:22
  29.7 1.9 copy-start.6
  31.6 2.5 copy-start.4
  34.3 3.6 copy-start.5
  42.6 17.4 %copy-start.3 = (bf16[1024,2048]{1,0:T(8,128)(2,1)S(1)}, bf16[1024,2048]{1,0:T(8,128)(2,1)}, u32[]{:S(2)}) copy-start(bf16[1024,2048]{1,0:T(8,128)(2,1)} %param.15) | copy-start | bytes 12582916
  64.2 1.9 copy-start
  64.2 1.9 copy-start.8
  68.1 187.0 %all-gather.6.cloned.1.call-start = ((), (), s32[]{:S(2)}) async-start(), calls=%async_computation.3 | async-start | bytes 17825792 | tf_op jit(solution)/shard_map/all_gather | solution.py:102
  68.8 316.5 %all-gather.8.cloned.1.call-start = ((), (), s32[]{:S(2)}) async-start(), calls=%async_computation.4 | async-start | bytes 17825792 | tf_op jit(solution)/shard_map/all_gather | solution.py:103
  69.6 392.2 %reduce-scatter.2.cloned.1.call-start = ((), (), s32[]{:S(2)}) async-start(), calls=%async_computation.5 | async-start | bytes 6291456 | tf_op jit(solution)/shard_map/reduce_scatter | solution.py:122
  461.8 4.0 copy-start.1
  461.8 4.7 copy-start.2
  465.7 2.0 copy-start.9
Sparse Core Ops, SparseCore 0:
  68.2 58.2 all-gather.3
  128.6 126.4 all-gather.5
  257.3 128.0 all-gather.7
  409.2 52.5 reduce-scatter.1
where the time goes:
time: 478 us
  waiting for transfers between devices  347 us (73%)
  matrix products  56.9 us (12%)
  other arithmetic  21.8 us (5%)
  blocking collectives  17.2 us (4%)
  between operations  13.4 us (3%)
  starting transfers between devices  10.9 us (2%)
  local copies, waits for them, and re-layouts  10.6 us (2%)
    all_gather x1, waiting for transfers between devices, per_device(): up_whole = lax.all_gather(up_weight, 'sp', axis=0, tiled=True)  129 us
    all_gather x1, waiting for transfers between devices, per_device(): down_whole = lax.all_gather(down_weight, 'sp', axis=1, tiled=True)  107 us
    all_gather x1, waiting for transfers between devices, per_device(): lax.all_gather(first_stream, 'tp', axis=0, tiled=True)  56.9 us
    reduce_scatter x1, waiting for transfers between devices, per_device(): lax.psum_scatter(jnp.dot(active, down_whole, preferred_element_type=jnp.f...  52.7 us
    dot_general x1, matrix products, per_device(): jnp.dot(active, down_whole, preferred_element_type=jnp.float32)  23.7 us
    dot_general x1, matrix products, per_device(): jnp.dot(lax.all_gather(first_stream, 'tp', axis=0, tiled=True), up_whole,...  22.9 us
    all_to_all x1, blocking collectives, per_device(): lax.all_to_all(by_peer, 'tp', split_axis=0, concat_axis=2, tiled=True)[0]  17.2 us
  transfers between devices with their start and end apart: 8, of which 4 were waited for; matrix products, arithmetic and copies ran while one was open for 7% of the time, Pallas kernels for 0%

commit v1 on v0

--- a/solution.py
+++ b/solution.py
@@ -1,6 +1,10 @@
+import functools
+
 import jax
 import jax.numpy as jnp
 from jax import lax
+from jax.experimental import pallas as pl
+from jax.experimental.pallas import tpu as pltpu
 from jax.sharding import PartitionSpec as P
 
 HEAD_SIZE = 64
@@ -130,9 +134,392 @@
     )
 
 
+def attend_body(kv_heads, total_rows, place, sinks, query, low, own, high, out, band, held, probs):
+    reach = WINDOW_REACH
+    tok_rows = own.shape[0]
+    unit = 2 * HEAD_SIZE
+    step = pl.program_id(0)
+    block = place[0] + step
+
+    @pl.when(step == 0)
+    def _():
+        band[:reach] = low[...]
+        band[reach : reach + tok_rows] = own[...]
+        band[reach + tok_rows :] = high[...]
+
+    start = pl.multiple_of(block * reach, reach)
+    marks = slice(kv_heads * unit, (kv_heads + 1) * unit)
+    key_docs = band[pl.ds(start, 3 * reach), marks].astype(jnp.float32).T
+    query_docs = band[pl.ds(start + reach, reach), marks].astype(jnp.float32)
+    shape = (reach, 3 * reach)
+    row = lax.broadcasted_iota(jnp.int32, shape, 0)
+    column = lax.broadcasted_iota(jnp.int32, shape, 1) - reach
+    key_pos = place[1] + start + column
+    allowed = (
+        (jnp.abs(row - column) <= reach)
+        & (key_pos >= 0)
+        & (key_pos < total_rows)
+        & (key_docs[:reach] == jnp.concatenate([query_docs] * 3, axis=1))
+    )
+    key_lanes = lax.broadcasted_iota(jnp.int32, (2 * reach, unit), 1) < HEAD_SIZE
+    scale = jnp.array(HEAD_SIZE**-0.5, query.dtype)
+    for head in range(kv_heads):
+        pair = band[pl.ds(start, 3 * reach), head * unit : (head + 1) * unit]
+        first = query[:, head * unit : (head + 1) * unit] * scale
+        second = jnp.concatenate([first[:, HEAD_SIZE:], first[:, :HEAD_SIZE]], axis=1)
+        both = jnp.concatenate([first, second], axis=0)
+        both = jnp.where(key_lanes, both, jnp.zeros_like(both))
+        scores = lax.dot_general(
+            both, pair, (((1,), (1,)), ((), ())), preferred_element_type=jnp.float32
+        )
+        for member in range(2):
+            part = scores[member * reach : (member + 1) * reach]
+            held[2 * head + member] = jnp.where(allowed, part, NEG_LARGE)
+    for number in range(2 * kv_heads):
+        scores = held[number]
+        sink = sinks[number]
+        highest = jnp.maximum(jnp.max(scores, axis=-1, keepdims=True), sink)
+        powers = jnp.exp(scores - highest)
+        denominator = jnp.sum(powers, axis=-1, keepdims=True) + jnp.exp(sink - highest)
+        at = slice((number % 2) * reach, (number % 2 + 1) * reach)
+        probs[number // 2, at] = (powers * (1.0 / denominator)).astype(probs.dtype)
+    for head in range(kv_heads):
+        pair = band[pl.ds(start, 3 * reach), head * unit : (head + 1) * unit]
+        mixed = jnp.dot(probs[head], pair, preferred_element_type=jnp.float32)
+        first = pltpu.roll(mixed[:reach], HEAD_SIZE, 1)
+        joined = jnp.where(key_lanes[:reach], first, mixed[reach:])
+        out[:, head * unit : (head + 1) * unit] = joined.astype(out.dtype)
+
+
+def attend_rows(kv_heads, total_rows, place, sinks, queries, low, own, high, rows):
+    reach = WINDOW_REACH
+    width = queries.shape[1]
+    whole = lambda array: pl.BlockSpec(array.shape, lambda n, place, sinks: (0, 0))
+    return pl.pallas_call(
+        functools.partial(attend_body, kv_heads, total_rows),
+        grid_spec=pltpu.PrefetchScalarGridSpec(
+            num_scalar_prefetch=2,
+            grid=(rows // reach,),
+            in_specs=[
+                pl.BlockSpec((reach, width), lambda n, place, sinks: (place[0] + n, 0)),
+                whole(low),
+                whole(own),
+                whole(high),
+            ],
+            out_specs=pl.BlockSpec((reach, width), lambda n, place, sinks: (n, 0)),
+            scratch_shapes=[
+                pltpu.VMEM((own.shape[0] + 2 * reach, own.shape[1]), own.dtype),
+                pltpu.VMEM((2 * kv_heads, reach, 3 * reach), jnp.float32),
+                pltpu.VMEM((kv_heads, 2 * reach, 3 * reach), own.dtype),
+            ],
+        ),
+        out_shape=jax.ShapeDtypeStruct((rows, width), queries.dtype),
+        cost_estimate=pl.CostEstimate(
+            flops=12 * rows * width * reach * 10, bytes_accessed=rows * width * 8, transcendentals=0
+        ),
+        name="attend_rows",
+    )(place, sinks, queries, low, own, high)
+
+
+def line_shape(mesh):
+    devices = mesh.devices
+    names = list(mesh.axis_names)
+    if names != ["sp", "tp"]:
+        return None
+    count, tp_count = devices.shape
+    where = [(*devices[i, 0].coords, devices[i, 0].core_on_chip) for i in range(count)]
+    zs = sorted({w[2] for w in where})
+    ys = sorted({w[1] for w in where})
+    cores = sorted({w[3] for w in where})
+    expected = [(where[0][0], y, z, c) for z in zs for y in ys for c in cores]
+    if where != expected or tp_count != 2 or (len(zs), len(ys), len(cores)) != (4, 2, 2):
+        return None
+    return len(zs), len(ys), len(cores)
+
+
+def up_body(tile, unit, order, *rest):
+    count = order.shape[0]
+    rows = rest[:4]
+    weights = rest[4 : 4 + count]
+    outs = rest[4 + count : 7 + count]
+    buffer, sems = rest[7 + count :]
+    step = pl.program_id(0)
+    steps = pl.num_programs(0)
+
+    def copies(index, slot):
+        return [
+            pltpu.make_async_copy(
+                weight.at[:, pl.ds(pl.multiple_of(index * tile, tile), tile)],
+                buffer.at[
+                    slot, pl.ds(pl.multiple_of(order[j] * unit, unit), weight.shape[0]), :
+                ],
+                sems.at[slot, j],
+            )
+            for j, weight in enumerate(weights)
+        ]
+
+    slot = lax.rem(step, 2)
+
+    @pl.when(step == 0)
+    def _():
+        for copy in copies(step, slot):
+            copy.start()
+
+    @pl.when(step + 1 < steps)
+    def _():
+        for copy in copies(step + 1, 1 - slot):
+            copy.start()
+
+    for copy in copies(step, slot):
+        copy.wait()
+    size = rows[0].shape[0]
+    places = ((outs[0], 0), (outs[0], size), (outs[1], 0), (outs[2], 0))
+    for part, (out, first) in zip(rows, places):
+        hidden = jnp.dot(part[...], buffer[slot], preferred_element_type=jnp.float32)
+        out[first : first + size] = jnp.square(jnp.maximum(hidden, 0.0)).astype(out.dtype)
+
+
+def up_project(order, rows, weights):
+    hidden_units = weights[0].shape[1]
+    unit = min(weight.shape[0] for weight in weights)
+    tile = min(512, hidden_units)
+    count, width = rows[0].shape
+    dtype = rows[0].dtype
+    return pl.pallas_call(
+        functools.partial(up_body, tile, unit),
+        grid_spec=pltpu.PrefetchScalarGridSpec(
+            num_scalar_prefetch=1,
+            grid=(hidden_units // tile,),
+            in_specs=[pl.BlockSpec((count, width), lambda n, order: (0, 0))] * 4
+            + [pl.BlockSpec(memory_space=pl.ANY)] * len(weights),
+            out_specs=[
+                pl.BlockSpec((size, tile), lambda n, order: (0, n))
+                for size in (2 * count, count, count)
+            ],
+            scratch_shapes=[
+                pltpu.VMEM((2, width, tile), dtype),
+                pltpu.SemaphoreType.DMA((2, len(weights))),
+            ],
+        ),
+        out_shape=[
+            jax.ShapeDtypeStruct((size, hidden_units), dtype) for size in (2 * count, count, count)
+        ],
+        cost_estimate=pl.CostEstimate(
+            flops=8 * count * width * hidden_units,
+            bytes_accessed=2 * width * hidden_units,
+            transcendentals=0,
+        ),
+        name="up_project",
+    )(order, *rows, *weights)
+
+
+def norm_body(parts, order, stream, gain, *rest):
+    mine = rest[:parts]
+    theirs = rest[parts : 2 * parts]
+    out, total = rest[2 * parts :]
+    block = 0
+    width = total.shape[1]
+    unit = width // order.shape[0]
+    for own, other in zip(mine, theirs):
+        for j in range(own.shape[1] // unit):
+            at = pl.ds(pl.multiple_of(order[block] * unit, unit), unit)
+            piece = slice(j * unit, (j + 1) * unit)
+            total[:, at] = own[:, piece].astype(jnp.float32) + other[:, piece].astype(jnp.float32)
+            block += 1
+    full = stream[...].astype(jnp.float32) + total[...]
+    out[...] = layer_norm(full, gain[...]).astype(out.dtype)
+
+
+def norm_sum(order, stream, gain, mine, theirs):
+    rows, width = stream.shape
+    tile = min(128, rows)
+    part_specs = [
+        pl.BlockSpec((tile, part.shape[1]), lambda n, order: (n, 0)) for part in [*mine, *theirs]
+    ]
+    return pl.pallas_call(
+        functools.partial(norm_body, len(mine)),
+        grid_spec=pltpu.PrefetchScalarGridSpec(
+            num_scalar_prefetch=1,
+            grid=(rows // tile,),
+            in_specs=[
+                pl.BlockSpec((tile, width), lambda n, order: (n, 0)),
+                pl.BlockSpec((1, width), lambda n, order: (0, 0)),
+                *part_specs,
+            ],
+            out_specs=pl.BlockSpec((tile, width), lambda n, order: (n, 0)),
+            scratch_shapes=[pltpu.VMEM((tile, width), jnp.float32)],
+        ),
+        out_shape=jax.ShapeDtypeStruct((rows, width), stream.dtype),
+        name="norm_sum",
+    )(order, stream, gain.reshape(1, width), *mine, *theirs)
+
+
+def per_device_line(
+    shape,
+    queries,
+    keyvals,
+    head_sink_logit,
+    doc_ids,
+    stream_in,
+    out_weight,
+    first_gain,
+    up_weight,
+    down_weight,
+    second_gain,
+):
+    nz, ny, nc = shape
+
+    def index(z, y, c):
+        return (z * ny + y) * nc + c
+
+    def pairs(target):
+        found = []
+        for z in range(nz):
+            for y in range(ny):
+                for c in range(nc):
+                    to = target(z, y, c)
+                    if to is not None:
+                        found.append((index(z, y, c), index(*to)))
+        return found
+
+    ring = [(z, 0) for z in range(nz)] + [(z, 1) for z in reversed(range(nz))]
+    chips = len(ring)
+
+    def turned(by):
+        return pairs(lambda z, y, c: (*ring[(ring.index((z, y)) + by) % chips], c))
+
+    onward = turned(1)
+    backward = turned(-1)
+    twin = pairs(lambda z, y, c: (z, y, 1 - c))
+    swap = [(0, 1), (1, 0)]
+
+    me = lax.axis_index("sp")
+    my_c = me % nc
+    my_y = (me // nc) % ny
+    my_z = me // (nc * ny)
+    tp_me = lax.axis_index("tp")
+
+    def send(value, way, axis="sp"):
+        return lax.ppermute(value, axis, way)
+
+    def halved(weight, hidden_axis):
+        half = weight.shape[hidden_axis] // nc
+        kept = lax.dynamic_slice_in_dim(weight, my_c * half, half, hidden_axis)
+        given = lax.dynamic_slice_in_dim(weight, (1 - my_c) * half, half, hidden_axis)
+        taken = send(given, twin)
+        low = jnp.where(my_c == 0, kept, taken)
+        high = jnp.where(my_c == 0, taken, kept)
+        return jnp.concatenate([low, high], axis=1 - hidden_axis)
+
+    def pass_on(left, right):
+        return send(left, onward), send(right, backward)
+
+    def half(block, number):
+        rows = block.shape[0] // 2
+        return lax.slice_in_dim(block, number * rows, (number + 1) * rows, axis=0)
+
+    up_own = halved(up_weight, 1)
+    up_blocks = [up_own]
+    left = right = up_own
+    for step in range(1, chips // 2):
+        left, right = pass_on(left, right)
+        up_blocks += [left, right]
+    up_blocks += pass_on(half(left, 0), half(right, 1))
+    down_own = halved(down_weight, 0)
+
+    place = jnp.where(my_y == 0, my_z, chips - 1 - my_z)
+
+    def chip_at(by):
+        at = (place + by) % chips
+        return jnp.where(at < nz, at * ny, (chips - 1 - at) * ny + 1)
+
+    steps = [0]
+    for step in range(1, chips // 2):
+        steps += [-step, step]
+    order = jnp.stack([chip_at(by) for by in (*steps, chips // 2)]).astype(jnp.int32)
+    last = 2 * order[-1:]
+    up_order = jnp.concatenate([2 * order[:-1], last, last + 1])
+
+    kv_heads = keyvals.shape[1]
+    tok_rows = queries.shape[0]
+    own_rows = tok_rows // 2
+    marked = jnp.concatenate(
+        [
+            keyvals.reshape(tok_rows, -1),
+            jnp.broadcast_to(doc_ids.astype(keyvals.dtype)[:, None], (tok_rows, keyvals.shape[2])),
+        ],
+        axis=1,
+    )
+    count = lax.axis_size("sp")
+    low = send(marked[-WINDOW_REACH:], [(i, i + 1) for i in range(count - 1)])
+    high = send(marked[:WINDOW_REACH], [(i + 1, i) for i in range(count - 1)])
+    blocks = own_rows // WINDOW_REACH
+
+    def attended(half):
+        place = jnp.stack([half * blocks, me * tok_rows]).astype(jnp.int32)
+        return attend_rows(
+            kv_heads, count * tok_rows, place, head_sink_logit, queries, low, marked, high, own_rows
+        )
+
+    given = attended(1 - tp_me)
+    taken = send(given, swap, "tp")
+    kept = attended(tp_me)
+    joined = jnp.concatenate(
+        [jnp.where(tp_me == 0, kept, taken), jnp.where(tp_me == 0, taken, kept)], axis=1
+    )
+    projected = jnp.dot(joined, out_weight, preferred_element_type=jnp.float32)
+    first_stream = layer_norm(stream_in.astype(jnp.float32) + projected, first_gain).astype(
+        jnp.bfloat16
+    )
+    peer_stream = send(first_stream, swap, "tp")
+    twin_stream = send(first_stream, twin)
+    far_stream = send(peer_stream, twin)
+    twin_active, own_active, peer_active = up_project(
+        up_order, (twin_stream, far_stream, first_stream, peer_stream), up_blocks
+    )
+
+    def after(value, *results):
+        return lax.optimization_barrier((value, *results))[0]
+
+    left, right = pass_on(down_own, down_own)
+    left, right = after(left, twin_active), after(right, twin_active)
+    column_blocks = [down_own]
+    mine, theirs = [], []
+    for number in range(chips):
+        step = (number + 1) // 2
+        if number % 2 == 1 and step < chips // 2:
+            column_blocks += [left, right]
+            if step + 1 < chips // 2:
+                left, right = pass_on(left, right)
+            else:
+                left, right = pass_on(half(left, 0), half(right, 1))
+        elif number == chips - 1:
+            column_blocks.append(jnp.concatenate([left, right], axis=0))
+        weight = column_blocks[number]
+        share = jnp.dot(twin_active, weight, preferred_element_type=jnp.float32).astype(
+            jnp.bfloat16
+        )
+        from_twin = send(share, twin).astype(jnp.float32)
+        to_peer = (
+            jnp.dot(peer_active, weight, preferred_element_type=jnp.float32)
+            + from_twin[own_rows:]
+        ).astype(jnp.bfloat16)
+        theirs.append(send(to_peer, swap, "tp"))
+        kept = (
+            jnp.dot(own_active, weight, preferred_element_type=jnp.float32)
+            + from_twin[:own_rows]
+        ).astype(jnp.bfloat16)
+        mine.append(kept)
+        if number % 2 == 0 and number > 0:
+            left, right = after(left, to_peer, kept), after(right, to_peer, kept)
+    return norm_sum(order, first_stream, second_gain, mine, theirs)
+
+
 def solution(mesh):
+    shape = line_shape(mesh)
+    body = per_device if shape is None else functools.partial(per_device_line, shape)
     return jax.shard_map(
-        per_device,
+        body,
         mesh=mesh,
         in_specs=(
             P("sp", "tp"),

time: 478 us -> 286 us (0.60)
  waiting for transfers between devices: 347 us -> 132 us
  Pallas kernels: 0 us -> 46 us
  starting transfers between devices: 10.9 us -> 41.2 us
  blocking collectives: 17.2 us -> 0 us
  matrix products: 56.9 us -> 43.2 us
  between operations: 13.4 us -> 0.93 us
  other arithmetic: 21.8 us -> 13.4 us
    all_gather x3 -> x0, waiting for transfers between devices: 293 us -> none  [the longest x1 129 us: per_device(): up_whole = lax.all_gather(up_weight, 'sp', axis=0, tiled=True)]
    ppermute x4 -> x40, waiting for transfers between devices: 0.01 us -> 132 us  [send(): return lax.ppermute(value, axis, way)]
    reduce_scatter x1 -> x0, waiting for transfers between devices: 52.7 us -> none  [per_device(): lax.psum_scatter(jnp.dot(active, down_whole, preferred_element_type=jnp.f...]
    pallas_call x0 -> x4, Pallas kernels: none -> 46 us  [the longest x1 25.1 us: up_project(): pl.pallas_call(functools.partial(up_body, tile, unit), grid_spec=pltpu.Pr...]
    ppermute x4 -> x40, starting transfers between devices: 10.8 us -> 41.2 us  [send(): return lax.ppermute(value, axis, way)]
    all_to_all x1 -> x0, blocking collectives: 17.2 us -> none  [per_device(): lax.all_to_all(by_peer, 'tp', split_axis=0, concat_axis=2, tiled=True)[0]]
    dot_general x5 -> x25, matrix products: 56.9 us -> 43.2 us  [the longest x8 15.6 us: per_device_line(): jnp.dot(twin_active, weight, preferred_element_type=jnp.float32)]
    reduce_sum x2 -> x0, other arithmetic: 7.36 us -> none  [the longest x1 3.93 us: layer_norm(): centre = jnp.mean(stream, axis=-1, keepdims=True)]
  transfers between devices with their start and end apart: 8 -> 40, of which waited for: 4 -> 16; matrix products, arithmetic and copies ran while one was open for 7% -> 21% of each run, Pallas kernels for 0% -> 11%
where the time goes in v1:
time: 286 us; the launch traced here: 285 us
  waiting for transfers between devices  132 us (46%)
  Pallas kernels  46 us (16%)
  matrix products  43.2 us (15%)
  starting transfers between devices  41.2 us (14%)
  other arithmetic  13.4 us (5%)
  local copies, waits for them, and re-layouts  8.32 us (3%)
    ppermute x40, waiting for transfers between devices, send(): return lax.ppermute(value, axis, way)  132 us
    ppermute x40, starting transfers between devices, send(): return lax.ppermute(value, axis, way)  41.2 us
    pallas_call x1, Pallas kernels, up_project(): pl.pallas_call(functools.partial(up_body, tile, unit), grid_spec=pltpu.Pr...  25.1 us
    dot_general x8, matrix products, per_device_line(): jnp.dot(twin_active, weight, preferred_element_type=jnp.float32)  15.6 us
    pallas_call x2, Pallas kernels, attend_rows(): pl.pallas_call(functools.partial(attend_body, kv_heads, total_rows), grid...  14.8 us
    dot_general x8, matrix products, per_device_line(): jnp.dot(own_active, weight, preferred_element_type=jnp.float32)  14.7 us
    dot_general x8, matrix products, per_device_line(): jnp.dot(peer_active, weight, preferred_element_type=jnp.float32)  8.3 us
    pallas_call x1, Pallas kernels, norm_sum(): pl.pallas_call(functools.partial(norm_body, len(mine)), grid_spec=pltpu.P...  6.11 us
  transfers between devices with their start and end apart: 40, of which 16 were waited for; matrix products, arithmetic and copies ran while one was open for 21% of the time, Pallas kernels for 11%

profile of v1, /device:TPU:0, one launch (start us, length us, event | category | flops | bytes accessed | tf_op | source)
XLA Modules:
  0.0 285.4 jit_solution(17521212207505203856)
XLA Ops:
  10.8 7.4 %attend_rows.3 = bf16[512,512]{1,0:T(8,128)(2,1)} custom-call(s32[2]{0:T(128)} %pad_add_fusion.1.place, f32[8]{0:T(128)} %sinks.3, bf16[1024,512]{1,0:T(8,128)(2,1)} %query.3, bf16[128,640]{1,0:T(8,128)(2,1)} %copy-done.18, bf16[1024,640]{1,0:T(8,128)(2,1)} %pad_maximum_fusion.own, bf16[128,640]{1,0:T(8,128)(2,1)} %copy-done.19), custom_call_target="tpu_custom_call" | custom-call | flops 4026531840 | bytes 2097152 | tf_op jit(solution)/shard_map/attend_rows/pallas_call | solution.py:198
  20.5 3.6 %collective-permute-start.6 = (bf16[128,2048]{1,0:T(8,128)(2,1)}, bf16[128,2048]{1,0:T(8,128)(2,1)}, u32[]{:S(2)}, u32[]{:S(2)}) collective-permute-start(bf16[128,2048]{1,0:T(8,128)(2,1)} %constant_dynamic-slice_fusion.1), channel_id=1, source_target_pairs={{0,2},{2,0},{4,6},{6,4},{8,10},{10,8},{12,14},{14,12},{16,18},{18,... | collective-permute-start | bytes 1572872 | tf_op jit(solution)/shard_map/ppermute | solution.py:403
  24.7 7.4 %attend_rows.2 = bf16[512,512]{1,0:T(8,128)(2,1)} custom-call(s32[2]{0:T(128)} %pad_add_fusion.place, f32[8]{0:T(128)} %sinks.3, bf16[1024,512]{1,0:T(8,128)(2,1)} %query.3, bf16[128,640]{1,0:T(8,128)(2,1)} %copy-done.18, bf16[1024,640]{1,0:T(8,128)(2,1)} %pad_maximum_fusion.own, bf16[128,640]{1,0:T(8,128)(2,1)} %copy-done.19), custom_call_target="tpu_custom_call" | custom-call | flops 4026531840 | bytes 2097152 | tf_op jit(solution)/shard_map/attend_rows/pallas_call | solution.py:198
  33.8 4.6 %fusion.22 = (f32[512]{0:T(512)S(1)}, f32[512,2048]{1,0:T(8,128)S(1)}) fusion(bf16[1024,2048]{1,0:T(8,128)(2,1)} %param.15, bf16[512,512]{1,0:T(8,128)(2,1)S(1)} %get-tuple-element.34, bf16[512,512]{1,0:T(8,128)(2,1)S(1)} %get-tuple-element.33, bf16[512,2048]{1,0:T(8,128)(2,1)S(1)} %copy-done.13), kind=kOutput, calls=%fused_computation.73 | convolution fusion | flops 2152726016 | bytes 11536384 | tf_op jit(solution)/shard_map/dot_general | solution.py:470
  42.3 5.6 %collective-permute-start.7 = (bf16[256,2048]{1,0:T(8,128)(2,1)S(1)}, bf16[256,2048]{1,0:T(8,128)(2,1)S(1)}, u32[]{:S(2)}, u32[]{:S(2)}) collective-permute-start(bf16[256,2048]{1,0:T(8,128)(2,1)S(1)} %pad_maximum_fusion.1.rest_4_), channel_id=1, source_target_pairs={{0,8},{2,10},{4,0},{6,2},{8,16},{10,18},{12,4},{14,6},{16,24},{18,... | collective-permute-start | bytes 3145736 | tf_op jit(solution)/shard_map/ppermute | solution.py:403
  47.8 22.3 %collective-permute-done.7.rest_5_ = bf16[256,2048]{1,0:T(8,128)(2,1)S(1)} collective-permute-done((bf16[256,2048]{1,0:T(8,128)(2,1)S(1)}, bf16[256,2048]{1,0:T(8,128)(2,1)S(1)}, u32[]{:S(2)}, u32[]{:S(2)}) %collective-permute-start.7) | collective-permute-done | bytes 1048608 | tf_op jit(solution)/shard_map/ppermute | solution.py:403
  70.1 2.5 collective-permute-start.9
  72.7 15.1 %collective-permute-done.4.rest_3_ = bf16[512,2048]{1,0:T(8,128)(2,1)} collective-permute-done((bf16[512,2048]{1,0:T(8,128)(2,1)S(1)}, bf16[512,2048]{1,0:T(8,128)(2,1)}, u32[]{:S(2)}, u32[]{:S(2)}) %collective-permute-start.4) | collective-permute-done | bytes 2097184 | tf_op jit(solution)/shard_map/ppermute | solution.py:403
  87.9 7.0 %collective-permute-done.9.rest_7_ = bf16[256,2048]{1,0:T(8,128)(2,1)} collective-permute-done((bf16[256,2048]{1,0:T(8,128)(2,1)S(1)}, bf16[256,2048]{1,0:T(8,128)(2,1)}, u32[]{:S(2)}, u32[]{:S(2)}) %collective-permute-start.9) | collective-permute-done | bytes 1048608 | tf_op jit(solution)/shard_map/ppermute | solution.py:403
  98.0 21.9 %collective-permute-done.11.rest_9_ = bf16[256,2048]{1,0:T(8,128)(2,1)} collective-permute-done((bf16[256,2048]{1,0:T(8,128)(2,1)}, bf16[256,2048]{1,0:T(8,128)(2,1)}, u32[]{:S(2)}, u32[]{:S(2)}) %collective-permute-start.11) | collective-permute-done | bytes 1048608 | tf_op jit(solution)/shard_map/ppermute | solution.py:403
  128.8 7.0 %collective-permute-done.13.rest_11_ = bf16[128,2048]{1,0:T(8,128)(2,1)S(1)} collective-permute-done((bf16[128,2048]{1,0:T(8,128)(2,1)S(1)}, bf16[128,2048]{1,0:T(8,128)(2,1)S(1)}, u32[]{:S(2)}, u32[]{:S(2)}) %collective-permute-start.13) | collective-permute-done | bytes 524320 | tf_op jit(solution)/shard_map/ppermute | solution.py:403
  138.2 25.1 %up_project.1 = (bf16[1024,2048]{1,0:T(8,128)(2,1)}, bf16[512,2048]{1,0:T(8,128)(2,1)}, bf16[512,2048]{1,0:T(8,128)(2,1)}) custom-call(s32[9]{0:T(128)} %pad_add_fusion.2.order, bf16[512,2048]{1,0:T(8,128)(2,1)} %collective-permute-done.3.rest_0_, bf16[512,2048]{1,0:T(8,128)(2,1)} %collective-permute-done.5.rest_1_, bf16[512,2048]{1,0:T(8,128)(2,1)} %copy-done, ...), custom_call_target="tpu_custom_call" | custom-call | flops 17179869184 | bytes 8388608 | tf_op jit(solution)/shard_map/up_project/pallas_call | solution.py:288
  163.3 3.6 %convolution_convert_fusion.7 = bf16[1024,256]{1,0:T(8,128)(2,1)S(1)} fusion(bf16[1024,2048]{1,0:T(8,128)(2,1)} %get-tuple-element.17, bf16[2048,128]{1,0:T(8,128)(2,1)S(1)} %get-tuple-element.28, bf16[2048,128]{1,0:T(8,128)(2,1)S(1)} %get-tuple-element.27), kind=kOutput, calls=%fused_computation.13 | convolution fusion | flops 1076101120 | bytes 5767168 | tf_op jit(solution)/shard_map/dot_general | solution.py:499
  170.0 3.3 %convolution_convert_fusion.5 = bf16[1024,256]{1,0:T(8,128)(2,1)} fusion(bf16[1024,2048]{1,0:T(8,128)(2,1)S(1)} %copy-done.22, bf16[2048,256]{1,0:T(8,128)(2,1)} %collective-permute-done.19), kind=kOutput, calls=%fused_computation.11 | convolution fusion | flops 1074003968 | bytes 5767168 | tf_op jit(solution)/shard_map/dot_general | solution.py:499
  176.1 3.3 %fusion.1.rest_1_ = bf16[512,256]{1,0:T(8,128)(2,1)} fusion(bf16[512,2048]{1,0:T(8,128)(2,1)} %get-tuple-element.16, bf16[2048,256]{1,0:T(8,128)(2,1)} %collective-permute-done.17, f32[1024,256]{1,0:T(8,128)S(1)} %convert_element_type.112), kind=kOutput, calls=%fused_computation.33 | convolution fusion | flops 537133056 | bytes 3932160 | tf_op jit(solution)/shard_map/dot_general | solution.py:509
  181.8 2.8 fusion.2.rest_2_
  188.6 11.1 %collective-permute-done.21 = bf16[2048,256]{1,0:T(8,128)(2,1)S(1)} collective-permute-done((bf16[2048,256]{1,0:T(8,128)(2,1)}, bf16[2048,256]{1,0:T(8,128)(2,1)S(1)}, u32[]{:S(2)}, u32[]{:S(2)}) %collective-permute-start.21) | collective-permute-done | bytes 1048608 | tf_op jit(solution)/shard_map/ppermute | solution.py:403
  214.8 14.6 %collective-permute-done.27 = bf16[2048,256]{1,0:T(8,128)(2,1)S(1)} collective-permute-done((bf16[2048,256]{1,0:T(8,128)(2,1)S(1)}, bf16[2048,256]{1,0:T(8,128)(2,1)S(1)}, u32[]{:S(2)}, u32[]{:S(2)}) %collective-permute-start.27) | collective-permute-done | bytes 1048608 | tf_op jit(solution)/shard_map/ppermute | solution.py:403
  231.5 2.6 collective-permute-done.25
  239.8 6.3 %collective-permute-done.29 = bf16[1024,256]{1,0:T(8,128)(2,1)S(1)} collective-permute-done((bf16[1024,256]{1,0:T(8,128)(2,1)S(1)}, bf16[1024,256]{1,0:T(8,128)(2,1)S(1)}, u32[]{:S(2)}, u32[]{:S(2)}) %collective-permute-start.29) | collective-permute-done | bytes 524320 | tf_op jit(solution)/shard_map/ppermute | solution.py:403
  259.3 2.8 collective-permute-done.35.rest_11_
  262.1 11.2 %collective-permute-done.37.rest_13_ = bf16[512,256]{1,0:T(8,128)(2,1)S(1)} collective-permute-done((bf16[512,256]{1,0:T(8,128)(2,1)S(1)}, bf16[512,256]{1,0:T(8,128)(2,1)S(1)}, u32[]{:S(2)}, u32[]{:S(2)}) %collective-permute-start.37) | collective-permute-done | bytes 262176 | tf_op jit(solution)/shard_map/ppermute | solution.py:403
  273.3 5.1 %collective-permute-done.39.rest_15_ = bf16[512,256]{1,0:T(8,128)(2,1)S(1)} collective-permute-done((bf16[512,256]{1,0:T(8,128)(2,1)S(1)}, bf16[512,256]{1,0:T(8,128)(2,1)S(1)}, u32[]{:S(2)}, u32[]{:S(2)}) %collective-permute-start.39) | collective-permute-done | bytes 262176 | tf_op jit(solution)/shard_map/ppermute | solution.py:403
  279.1 6.1 %norm_sum.1 = bf16[512,2048]{1,0:T(8,128)(2,1)} custom-call(s32[8]{0:T(128)} %stack.53.order, bf16[512,2048]{1,0:T(8,128)(2,1)} %copy-done, f32[1,2048]{1,0:T(1,128)} %bitcast.65, bf16[512,256]{1,0:T(8,128)(2,1)} %fusion.rest_0_, bf16[512,256]{1,0:T(8,128)(2,1)} %fusion.1.rest_1_, bf16[512,256]{1,0:T(8,128)(2,1)} %fusion.2.rest_2_, ...), custom_call_target="tpu_custom_call" | custom-call | tf_op jit(solution)/shard_map/norm_sum/pallas_call | solution.py:339
  (169 shorter events, 82.2 us)
Async XLA Ops:
  20.5 19.9 %collective-permute-start.6 = (bf16[128,2048]{1,0:T(8,128)(2,1)}, bf16[128,2048]{1,0:T(8,128)(2,1)}, u32[]{:S(2)}, u32[]{:S(2)}) collective-permute-start(bf16[128,2048]{1,0:T(8,128)(2,1)} %constant_dynamic-slice_fusion.1), channel_id=1, source_target_pairs={{0,2},{2,0},{4,6},{6,4},{8,10},{10,8},{12,14},{14,12},{16,18},{18,... | collective-permute-start | bytes 1572872 | tf_op jit(solution)/shard_map/ppermute | solution.py:403
  39.8 48.1 %collective-permute-start.4 = (bf16[512,2048]{1,0:T(8,128)(2,1)S(1)}, bf16[512,2048]{1,0:T(8,128)(2,1)}, u32[]{:S(2)}, u32[]{:S(2)}) collective-permute-start(bf16[512,2048]{1,0:T(8,128)(2,1)S(1)} %multiply_convert_fusion.rest_2_.stream), channel_id=1, source_target_pairs={{0,1},{1,0},{2,3},{3,2},{4,5},{5,4},{6,7},{7,6},{8,9},{9,8},{10,11... | collective-permute-start | bytes 6291464 | tf_op jit(solution)/shard_map/ppermute | solution.py:403
  42.3 27.9 %collective-permute-start.7 = (bf16[256,2048]{1,0:T(8,128)(2,1)S(1)}, bf16[256,2048]{1,0:T(8,128)(2,1)S(1)}, u32[]{:S(2)}, u32[]{:S(2)}) collective-permute-start(bf16[256,2048]{1,0:T(8,128)(2,1)S(1)} %pad_maximum_fusion.1.rest_4_), channel_id=1, source_target_pairs={{0,8},{2,10},{4,0},{6,2},{8,16},{10,18},{12,4},{14,6},{16,24},{18,... | collective-permute-start | bytes 3145736 | tf_op jit(solution)/shard_map/ppermute | solution.py:403
  47.8 24.8 %collective-permute-start.8 = (bf16[256,2048]{1,0:T(8,128)(2,1)S(1)}, bf16[256,2048]{1,0:T(8,128)(2,1)S(1)}, u32[]{:S(2)}, u32[]{:S(2)}) collective-permute-start(bf16[256,2048]{1,0:T(8,128)(2,1)S(1)} %pad_maximum_fusion.1.rest_4_), channel_id=1, source_target_pairs={{0,4},{2,6},{4,12},{6,14},{8,0},{10,2},{12,20},{14,22},{16,8},{18,... | collective-permute-start | bytes 3145736 | tf_op jit(solution)/shard_map/ppermute | solution.py:403
  70.1 24.7 %collective-permute-start.9 = (bf16[256,2048]{1,0:T(8,128)(2,1)S(1)}, bf16[256,2048]{1,0:T(8,128)(2,1)}, u32[]{:S(2)}, u32[]{:S(2)}) collective-permute-start(bf16[256,2048]{1,0:T(8,128)(2,1)S(1)} %collective-permute-done.7.rest_5_), channel_id=1, source_target_pairs={{0,8},{2,10},{4,0},{6,2},{8,16},{10,18},{12,4},{14,6},{16,24},{18,... | collective-permute-start | bytes 3145736 | tf_op jit(solution)/shard_map/ppermute | solution.py:403
  72.6 24.2 %collective-permute-start.10 = (bf16[256,2048]{1,0:T(8,128)(2,1)S(1)}, bf16[256,2048]{1,0:T(8,128)(2,1)}, u32[]{:S(2)}, u32[]{:S(2)}) collective-permute-start(bf16[256,2048]{1,0:T(8,128)(2,1)S(1)} %collective-permute-done.8.rest_6_), channel_id=1, source_target_pairs={{0,4},{2,6},{4,12},{6,14},{8,0},{10,2},{12,20},{14,22},{16,8},{18,... | collective-permute-start | bytes 3145736 | tf_op jit(solution)/shard_map/ppermute | solution.py:403
  72.7 54.6 %collective-permute-start.3 = (bf16[512,2048]{1,0:T(8,128)(2,1)S(1)}, bf16[512,2048]{1,0:T(8,128)(2,1)}, u32[]{:S(2)}, u32[]{:S(2)}) collective-permute-start(bf16[512,2048]{1,0:T(8,128)(2,1)S(1)} %multiply_convert_fusion.rest_2_.stream), channel_id=1, source_target_pairs={{0,2},{2,0},{4,6},{6,4},{8,10},{10,8},{12,14},{14,12},{16,18},{18,... | collective-permute-start | bytes 6291464 | tf_op jit(solution)/shard_map/ppermute | solution.py:403
  87.9 50.3 %collective-permute-start.5 = (bf16[512,2048]{1,0:T(8,128)(2,1)}, bf16[512,2048]{1,0:T(8,128)(2,1)}, u32[]{:S(2)}, u32[]{:S(2)}) collective-permute-start(bf16[512,2048]{1,0:T(8,128)(2,1)} %collective-permute-done.4.rest_3_), channel_id=1, source_target_pairs={{0,2},{2,0},{4,6},{6,4},{8,10},{10,8},{12,14},{14,12},{16,18},{18,... | collective-permute-start | bytes 6291464 | tf_op jit(solution)/shard_map/ppermute | solution.py:403
  94.9 25.0 %collective-permute-start.11 = (bf16[256,2048]{1,0:T(8,128)(2,1)}, bf16[256,2048]{1,0:T(8,128)(2,1)}, u32[]{:S(2)}, u32[]{:S(2)}) collective-permute-start(bf16[256,2048]{1,0:T(8,128)(2,1)} %collective-permute-done.9.rest_7_), channel_id=1, source_target_pairs={{0,8},{2,10},{4,0},{6,2},{8,16},{10,18},{12,4},{14,6},{16,24},{18,... | collective-permute-start | bytes 3145736 | tf_op jit(solution)/shard_map/ppermute | solution.py:403
  96.8 24.7 %collective-permute-start.12 = (bf16[256,2048]{1,0:T(8,128)(2,1)}, bf16[256,2048]{1,0:T(8,128)(2,1)}, u32[]{:S(2)}, u32[]{:S(2)}) collective-permute-start(bf16[256,2048]{1,0:T(8,128)(2,1)} %collective-permute-done.10.rest_8_), channel_id=1, source_target_pairs={{0,4},{2,6},{4,12},{6,14},{8,0},{10,2},{12,20},{14,22},{16,8},{18,... | collective-permute-start | bytes 3145736 | tf_op jit(solution)/shard_map/ppermute | solution.py:403
  97.0 27.3 %collective-permute-start.15 = (bf16[2048,128]{1,0:T(8,128)(2,1)S(1)}, bf16[2048,128]{1,0:T(8,128)(2,1)}, u32[]{:S(2)}, u32[]{:S(2)}) collective-permute-start(bf16[2048,128]{1,0:T(8,128)(2,1)S(1)} %constant_dynamic-slice_fusion), channel_id=1, source_target_pairs={{0,2},{2,0},{4,6},{6,4},{8,10},{10,8},{12,14},{14,12},{16,18},{18,... | collective-permute-start | bytes 1572872 | tf_op jit(solution)/shard_map/ppermute | solution.py:403
  126.8 40.1 %collective-permute-start.17 = (bf16[2048,256]{1,0:T(8,128)(2,1)}, bf16[2048,256]{1,0:T(8,128)(2,1)}, u32[]{:S(2)}, u32[]{:S(2)}) collective-permute-start(bf16[2048,256]{1,0:T(8,128)(2,1)} %pad_maximum_fusion.2), channel_id=1, source_target_pairs={{0,8},{2,10},{4,0},{6,2},{8,16},{10,18},{12,4},{14,6},{16,24},{18,... | collective-permute-start | bytes 3145736 | tf_op jit(solution)/shard_map/ppermute | solution.py:403
  127.2 42.8 %collective-permute-start.19 = (bf16[2048,256]{1,0:T(8,128)(2,1)}, bf16[2048,256]{1,0:T(8,128)(2,1)}, u32[]{:S(2)}, u32[]{:S(2)}) collective-permute-start(bf16[2048,256]{1,0:T(8,128)(2,1)} %pad_maximum_fusion.2), channel_id=1, source_target_pairs={{0,4},{2,6},{4,12},{6,14},{8,0},{10,2},{12,20},{14,22},{16,8},{18,... | collective-permute-start | bytes 3145736 | tf_op jit(solution)/shard_map/ppermute | solution.py:403
  174.0 25.8 %collective-permute-start.21 = (bf16[2048,256]{1,0:T(8,128)(2,1)}, bf16[2048,256]{1,0:T(8,128)(2,1)S(1)}, u32[]{:S(2)}, u32[]{:S(2)}) collective-permute-start(bf16[2048,256]{1,0:T(8,128)(2,1)} %collective-permute-done.17), channel_id=1, source_target_pairs={{0,8},{2,10},{4,0},{6,2},{8,16},{10,18},{12,4},{14,6},{16,24},{18,... | collective-permute-start | bytes 3145736 | tf_op jit(solution)/shard_map/ppermute | solution.py:403
  175.5 25.5 %collective-permute-start.23 = (bf16[2048,256]{1,0:T(8,128)(2,1)}, bf16[2048,256]{1,0:T(8,128)(2,1)S(1)}, u32[]{:S(2)}, u32[]{:S(2)}) collective-permute-start(bf16[2048,256]{1,0:T(8,128)(2,1)} %collective-permute-done.19), channel_id=1, source_target_pairs={{0,4},{2,6},{4,12},{6,14},{8,0},{10,2},{12,20},{14,22},{16,8},{18,... | collective-permute-start | bytes 3145736 | tf_op jit(solution)/shard_map/ppermute | solution.py:403
  204.3 25.1 %collective-permute-start.27 = (bf16[2048,256]{1,0:T(8,128)(2,1)S(1)}, bf16[2048,256]{1,0:T(8,128)(2,1)S(1)}, u32[]{:S(2)}, u32[]{:S(2)}) collective-permute-start(bf16[2048,256]{1,0:T(8,128)(2,1)S(1)} %collective-permute-done.23), channel_id=1, source_target_pairs={{0,4},{2,6},{4,12},{6,14},{8,0},{10,2},{12,20},{14,22},{16,8},{18,... | collective-permute-start | bytes 3145736 | tf_op jit(solution)/shard_map/ppermute | solution.py:403
  206.6 51.0 %collective-permute-start.34 = (bf16[512,256]{1,0:T(8,128)(2,1)S(1)}, bf16[512,256]{1,0:T(8,128)(2,1)S(1)}, u32[]{:S(2)}, u32[]{:S(2)}) collective-permute-start(bf16[512,256]{1,0:T(8,128)(2,1)S(1)} %fusion.3), channel_id=1, source_target_pairs={{0,1},{1,0},{2,3},{3,2},{4,5},{5,4},{6,7},{7,6},{8,9},{9,8},{10,11... | collective-permute-start | bytes 786440 | tf_op jit(solution)/shard_map/ppermute | solution.py:403
  208.0 47.6 %collective-permute-start.32 = (bf16[512,256]{1,0:T(8,128)(2,1)S(1)}, bf16[512,256]{1,0:T(8,128)(2,1)S(1)}, u32[]{:S(2)}, u32[]{:S(2)}) collective-permute-start(bf16[512,256]{1,0:T(8,128)(2,1)S(1)} %fusion.11), channel_id=1, source_target_pairs={{0,1},{1,0},{2,3},{3,2},{4,5},{5,4},{6,7},{7,6},{8,9},{9,8},{10,11... | collective-permute-start | bytes 786440 | tf_op jit(solution)/shard_map/ppermute | solution.py:403
  208.7 47.1 %collective-permute-start.33 = (bf16[512,256]{1,0:T(8,128)(2,1)S(1)}, bf16[512,256]{1,0:T(8,128)(2,1)S(1)}, u32[]{:S(2)}, u32[]{:S(2)}) collective-permute-start(bf16[512,256]{1,0:T(8,128)(2,1)S(1)} %fusion.12), channel_id=1, source_target_pairs={{0,1},{1,0},{2,3},{3,2},{4,5},{5,4},{6,7},{7,6},{8,9},{9,8},{10,11... | collective-permute-start | bytes 786440 | tf_op jit(solution)/shard_map/ppermute | solution.py:403
  210.1 24.0 %collective-permute-start.25 = (bf16[2048,256]{1,0:T(8,128)(2,1)S(1)}, bf16[2048,256]{1,0:T(8,128)(2,1)S(1)}, u32[]{:S(2)}, u32[]{:S(2)}) collective-permute-start(bf16[2048,256]{1,0:T(8,128)(2,1)S(1)} %collective-permute-done.21), channel_id=1, source_target_pairs={{0,8},{2,10},{4,0},{6,2},{8,16},{10,18},{12,4},{14,6},{16,24},{18,... | collective-permute-start | bytes 3145736 | tf_op jit(solution)/shard_map/ppermute | solution.py:403
  246.1 16.0 %collective-permute-start.36 = (bf16[512,256]{1,0:T(8,128)(2,1)S(1)}, bf16[512,256]{1,0:T(8,128)(2,1)S(1)}, u32[]{:S(2)}, u32[]{:S(2)}) collective-permute-start(bf16[512,256]{1,0:T(8,128)(2,1)S(1)} %fusion.6), channel_id=1, source_target_pairs={{0,1},{1,0},{2,3},{3,2},{4,5},{5,4},{6,7},{7,6},{8,9},{9,8},{10,11... | collective-permute-start | bytes 786440 | tf_op jit(solution)/shard_map/ppermute | solution.py:403
  255.6 17.8 %collective-permute-start.38 = (bf16[512,256]{1,0:T(8,128)(2,1)S(1)}, bf16[512,256]{1,0:T(8,128)(2,1)S(1)}, u32[]{:S(2)}, u32[]{:S(2)}) collective-permute-start(bf16[512,256]{1,0:T(8,128)(2,1)S(1)} %fusion.9), channel_id=1, source_target_pairs={{0,1},{1,0},{2,3},{3,2},{4,5},{5,4},{6,7},{7,6},{8,9},{9,8},{10,11... | collective-permute-start | bytes 786440 | tf_op jit(solution)/shard_map/ppermute | solution.py:403
  255.8 17.5 %collective-permute-start.37 = (bf16[512,256]{1,0:T(8,128)(2,1)S(1)}, bf16[512,256]{1,0:T(8,128)(2,1)S(1)}, u32[]{:S(2)}, u32[]{:S(2)}) collective-permute-start(bf16[512,256]{1,0:T(8,128)(2,1)S(1)} %fusion.14), channel_id=1, source_target_pairs={{0,1},{1,0},{2,3},{3,2},{4,5},{5,4},{6,7},{7,6},{8,9},{9,8},{10,11... | collective-permute-start | bytes 786440 | tf_op jit(solution)/shard_map/ppermute | solution.py:403
  257.7 20.8 %collective-permute-start.39 = (bf16[512,256]{1,0:T(8,128)(2,1)S(1)}, bf16[512,256]{1,0:T(8,128)(2,1)S(1)}, u32[]{:S(2)}, u32[]{:S(2)}) collective-permute-start(bf16[512,256]{1,0:T(8,128)(2,1)S(1)} %fusion.15), channel_id=1, source_target_pairs={{0,1},{1,0},{2,3},{3,2},{4,5},{5,4},{6,7},{7,6},{8,9},{9,8},{10,11... | collective-permute-start | bytes 786440 | tf_op jit(solution)/shard_map/ppermute | solution.py:403
  (40 other events, 420.6 us)

commit v2 on v1

--- a/solution.py
+++ b/solution.py
@@ -13,6 +13,9 @@
 
 NEG_LARGE = -1e30
 NORM_EPS = 1e-05
+
+VMEM_SMALL = 14 * 2**20
+VMEM_LARGE = 58 * 2**20
 
 
 def padded(block, sides, width):
@@ -217,6 +220,7 @@
         cost_estimate=pl.CostEstimate(
             flops=12 * rows * width * reach * 10, bytes_accessed=rows * width * 8, transcendentals=0
         ),
+        compiler_params=pltpu.CompilerParams(vmem_limit_bytes=VMEM_SMALL),
         name="attend_rows",
     )(place, sinks, queries, low, own, high)
 
@@ -309,8 +313,98 @@
             bytes_accessed=2 * width * hidden_units,
             transcendentals=0,
         ),
+        compiler_params=pltpu.CompilerParams(vmem_limit_bytes=VMEM_LARGE),
         name="up_project",
     )(order, *rows, *weights)
+
+
+def block_dots(rows, weights):
+    width = rows.shape[1]
+    if weights[0].shape[0] == width:
+        return [jnp.dot(rows[...], w[...], preferred_element_type=jnp.float32) for w in weights]
+    total, at = None, 0
+    for w in weights:
+        part = jnp.dot(
+            rows[:, at : at + w.shape[0]], w[...], preferred_element_type=jnp.float32
+        )
+        total = part if total is None else total + part
+        at += w.shape[0]
+    return [total]
+
+
+def share_body(count, rows, *rest):
+    out = rest[count]
+    at = 0
+    for part in block_dots(rows, rest[:count]):
+        out[:, at : at + part.shape[1]] = part.astype(out.dtype)
+        at += part.shape[1]
+
+
+def sum_body(count, peer, own, from_peer, from_own, *rest):
+    to_peer, kept = rest[count:]
+    for rows, extra, out in ((peer, from_peer, to_peer), (own, from_own, kept)):
+        at = 0
+        for part in block_dots(rows, rest[:count]):
+            columns = slice(at, at + part.shape[1])
+            out[:, columns] = (part + extra[:, columns].astype(jnp.float32)).astype(out.dtype)
+            at += part.shape[1]
+
+
+def columns_of(rows, weights):
+    whole = weights[0].shape[0] == rows.shape[1]
+    return weights[0].shape[1] * (len(weights) if whole else 1)
+
+
+def share_of(rows, weights):
+    count, width = rows.shape
+    tile = min(512, count)
+    columns = columns_of(rows, weights)
+    return pl.pallas_call(
+        functools.partial(share_body, len(weights)),
+        grid=(count // tile,),
+        in_specs=[
+            pl.BlockSpec((tile, width), lambda n: (n, 0)),
+            *(pl.BlockSpec(w.shape, lambda n: (0, 0)) for w in weights),
+        ],
+        out_specs=pl.BlockSpec((tile, columns), lambda n: (n, 0)),
+        out_shape=jax.ShapeDtypeStruct((count, columns), rows.dtype),
+        cost_estimate=pl.CostEstimate(
+            flops=2 * count * width * columns,
+            bytes_accessed=2 * (count + columns) * width,
+            transcendentals=0,
+        ),
+        compiler_params=pltpu.CompilerParams(vmem_limit_bytes=VMEM_SMALL),
+        name="share_of",
+    )(rows, *weights)
+
+
+def sum_of(peer, own, from_twin, weights):
+    count, width = own.shape
+    tile = min(256, count)
+    steps = count // tile
+    columns = columns_of(own, weights)
+    rows = pl.BlockSpec((tile, width), lambda n: (n, 0))
+    found = pl.BlockSpec((tile, columns), lambda n: (n, 0))
+    return pl.pallas_call(
+        functools.partial(sum_body, len(weights)),
+        grid=(steps,),
+        in_specs=[
+            rows,
+            rows,
+            pl.BlockSpec((tile, columns), lambda n: (n + steps, 0)),
+            found,
+            *(pl.BlockSpec(w.shape, lambda n: (0, 0)) for w in weights),
+        ],
+        out_specs=[found, found],
+        out_shape=[jax.ShapeDtypeStruct((count, columns), own.dtype)] * 2,
+        cost_estimate=pl.CostEstimate(
+            flops=4 * count * width * columns,
+            bytes_accessed=2 * (2 * count + columns) * width,
+            transcendentals=0,
+        ),
+        compiler_params=pltpu.CompilerParams(vmem_limit_bytes=VMEM_SMALL),
+        name="sum_of",
+    )(peer, own, from_twin, from_twin, *weights)
 
 
 def norm_body(parts, order, stream, gain, *rest):
@@ -350,6 +444,7 @@
             scratch_shapes=[pltpu.VMEM((tile, width), jnp.float32)],
         ),
         out_shape=jax.ShapeDtypeStruct((rows, width), stream.dtype),
+        compiler_params=pltpu.CompilerParams(vmem_limit_bytes=VMEM_SMALL),
         name="norm_sum",
     )(order, stream, gain.reshape(1, width), *mine, *theirs)
 
@@ -421,7 +516,7 @@
     up_own = halved(up_weight, 1)
     up_blocks = [up_own]
     left = right = up_own
-    for step in range(1, chips // 2):
+    for _ in range(1, chips // 2):
         left, right = pass_on(left, right)
         up_blocks += [left, right]
     up_blocks += pass_on(half(left, 0), half(right, 1))
@@ -483,35 +578,30 @@
 
     left, right = pass_on(down_own, down_own)
     left, right = after(left, twin_active), after(right, twin_active)
-    column_blocks = [down_own]
     mine, theirs = [], []
-    for number in range(chips):
-        step = (number + 1) // 2
-        if number % 2 == 1 and step < chips // 2:
-            column_blocks += [left, right]
-            if step + 1 < chips // 2:
-                left, right = pass_on(left, right)
-            else:
-                left, right = pass_on(half(left, 0), half(right, 1))
-        elif number == chips - 1:
-            column_blocks.append(jnp.concatenate([left, right], axis=0))
-        weight = column_blocks[number]
-        share = jnp.dot(twin_active, weight, preferred_element_type=jnp.float32).astype(
-            jnp.bfloat16
-        )
-        from_twin = send(share, twin).astype(jnp.float32)
-        to_peer = (
-            jnp.dot(peer_active, weight, preferred_element_type=jnp.float32)
-            + from_twin[own_rows:]
-        ).astype(jnp.bfloat16)
+
+    def share(weights):
+        given = share_of(twin_active, weights)
+        return send(given, twin)
+
+    def summed(from_twin, weights):
+        to_peer, kept = sum_of(peer_active, own_active, from_twin, weights)
+        mine.append(kept)
         theirs.append(send(to_peer, swap, "tp"))
-        kept = (
-            jnp.dot(own_active, weight, preferred_element_type=jnp.float32)
-            + from_twin[:own_rows]
-        ).astype(jnp.bfloat16)
-        mine.append(kept)
-        if number % 2 == 0 and number > 0:
-            left, right = after(left, to_peer, kept), after(right, to_peer, kept)
+        return to_peer
+
+    from_twin = share((down_own,))
+    for step in range(1, chips // 2 + 1):
+        pair = (left, right)
+        if step + 1 < chips // 2:
+            left, right = pass_on(left, right)
+        elif step + 1 == chips // 2:
+            left, right = pass_on(half(left, 0), half(right, 1))
+        from_twin_too = share(pair)
+        if step == 1:
+            summed(from_twin, (down_own,))
+        done = summed(from_twin_too, pair)
+        left, right = after(left, done), after(right, done)
     return norm_sum(order, first_stream, second_gain, mine, theirs)
 
 

time: 286 us -> 296 us (1.035)
  matrix products: 43.2 us -> 2.51 us
  waiting for transfers between devices: 132 us -> 168 us
  Pallas kernels: 46 us -> 63 us
  other arithmetic: 13.4 us -> 7.89 us
  local copies, waits for them, and re-layouts: 8.32 us -> 12.6 us
    dot_general x24 -> x0, matrix products: 38.5 us -> none  [the longest x8 15.6 us: per_device_line(): jnp.dot(twin_active, weight, preferred_element_type=jnp.float32)]
    ppermute x40 -> x34, waiting for transfers between devices: 132 us -> 168 us  [send(): return lax.ppermute(value, axis, way)]
    pallas_call x0 -> x10, Pallas kernels: none -> 22.6 us  [the longest x5 12.2 us: sum_of(): pl.pallas_call(functools.partial(sum_body, len(weights)), grid=(steps,),...]
    pallas_call x2, Pallas kernels: 14.8 us -> 10.2 us  [attend_rows(): pl.pallas_call(functools.partial(attend_body, kv_heads, total_rows), grid...]
    unnamed x50 -> x51, local copies, waits for them, and re-layouts: 4.25 us -> 8.3 us
    ppermute x40 -> x34, starting transfers between devices: 41.2 us -> 40.4 us  [send(): return lax.ppermute(value, axis, way)]
  transfers between devices with their start and end apart: 40 -> 34, of which waited for: 16 -> 18; matrix products, arithmetic and copies ran while one was open for 21% -> 5% of each run, Pallas kernels for 11% -> 15%
where the time goes in v2:
time: 296 us; the launch traced here: 295 us
  waiting for transfers between devices  168 us (57%)
  Pallas kernels  63 us (21%)
  starting transfers between devices  40.4 us (14%)
  local copies, waits for them, and re-layouts  12.6 us (4%)
  other arithmetic  7.89 us (3%)
    ppermute x34, waiting for transfers between devices, send(): return lax.ppermute(value, axis, way)  168 us
    ppermute x34, starting transfers between devices, send(): return lax.ppermute(value, axis, way)  40.4 us
    pallas_call x1, Pallas kernels, up_project(): pl.pallas_call(functools.partial(up_body, tile, unit), grid_spec=pltpu.Pr...  25 us
    pallas_call x5, Pallas kernels, sum_of(): pl.pallas_call(functools.partial(sum_body, len(weights)), grid=(steps,),...  12.2 us
    pallas_call x5, Pallas kernels, share_of(): pl.pallas_call(functools.partial(share_body, len(weights)), grid=(count /...  10.4 us
    pallas_call x2, Pallas kernels, attend_rows(): pl.pallas_call(functools.partial(attend_body, kv_heads, total_rows), grid...  10.2 us
    unnamed x51, local copies, waits for them, and re-layouts  8.3 us
  transfers between devices with their start and end apart: 34, of which 18 were waited for; matrix products, arithmetic and copies ran while one was open for 5% of the time, Pallas kernels for 15%

profile of v2, /device:TPU:0, one launch (start us, length us, event | category | flops | bytes accessed | tf_op | source)
XLA Modules:
  0.0 295.1 jit_solution(12789288861649173657)
XLA Ops:
  2.4 2.5 collective-permute-start
  7.7 2.7 collective-permute-done.1.high
  10.3 5.1 %attend_rows.3 = bf16[512,512]{1,0:T(8,128)(2,1)S(1)} custom-call(s32[2]{0:T(128)S(1)} %pad_add_fusion.1.place, f32[8]{0:T(128)S(1)} %copy-done.11, bf16[1024,512]{1,0:T(8,128)(2,1)S(1)} %copy-done.10, bf16[128,640]{1,0:T(8,128)(2,1)S(1)} %collective-permute-done.low, bf16[1024,640]{1,0:T(8,128)(2,1)S(1)} %pad_maximum_fusion.own, ...), custom_call_target="tpu_custom_call" | custom-call | flops 4026531840 | bytes 2097152 | tf_op jit(solution)/shard_map/attend_rows/pallas_call | solution.py:201
  17.9 3.6 %collective-permute-start.6 = (bf16[128,2048]{1,0:T(8,128)(2,1)}, bf16[128,2048]{1,0:T(8,128)(2,1)}, u32[]{:S(2)}, u32[]{:S(2)}) collective-permute-start(bf16[128,2048]{1,0:T(8,128)(2,1)} %constant_dynamic-slice_fusion.1), channel_id=1, source_target_pairs={{0,2},{2,0},{4,6},{6,4},{8,10},{10,8},{12,14},{14,12},{16,18},{18,... | collective-permute-start | bytes 1572872 | tf_op jit(solution)/shard_map/ppermute | solution.py:498
  21.5 5.1 %attend_rows.2 = bf16[512,512]{1,0:T(8,128)(2,1)S(1)} custom-call(s32[2]{0:T(128)S(1)} %pad_add_fusion.place, f32[8]{0:T(128)S(1)} %copy-done.11, bf16[1024,512]{1,0:T(8,128)(2,1)S(1)} %copy-done.10, bf16[128,640]{1,0:T(8,128)(2,1)S(1)} %collective-permute-done.low, bf16[1024,640]{1,0:T(8,128)(2,1)S(1)} %pad_maximum_fusion.own, ...), custom_call_target="tpu_custom_call" | custom-call | flops 4026531840 | bytes 2097152 | tf_op jit(solution)/shard_map/attend_rows/pallas_call | solution.py:201
  35.5 7.4 %collective-permute-start.7 = (bf16[256,2048]{1,0:T(8,128)(2,1)S(1)}, bf16[256,2048]{1,0:T(8,128)(2,1)S(1)}, u32[]{:S(2)}, u32[]{:S(2)}) collective-permute-start(bf16[256,2048]{1,0:T(8,128)(2,1)S(1)} %pad_maximum_fusion.1.rest_4_), channel_id=1, source_target_pairs={{0,8},{2,10},{4,0},{6,2},{8,16},{10,18},{12,4},{14,6},{16,24},{18,... | collective-permute-start | bytes 3145736 | tf_op jit(solution)/shard_map/ppermute | solution.py:498
  42.9 22.3 %collective-permute-done.7.rest_5_ = bf16[256,2048]{1,0:T(8,128)(2,1)S(1)} collective-permute-done((bf16[256,2048]{1,0:T(8,128)(2,1)S(1)}, bf16[256,2048]{1,0:T(8,128)(2,1)S(1)}, u32[]{:S(2)}, u32[]{:S(2)}) %collective-permute-start.7) | collective-permute-done | bytes 1048608 | tf_op jit(solution)/shard_map/ppermute | solution.py:498
  67.8 11.7 %collective-permute-done.4.rest_3_ = bf16[512,2048]{1,0:T(8,128)(2,1)} collective-permute-done((bf16[512,2048]{1,0:T(8,128)(2,1)S(1)}, bf16[512,2048]{1,0:T(8,128)(2,1)}, u32[]{:S(2)}, u32[]{:S(2)}) %collective-permute-start.4) | collective-permute-done | bytes 2097184 | tf_op jit(solution)/shard_map/ppermute | solution.py:498
  81.4 8.6 %collective-permute-done.9.rest_7_ = bf16[256,2048]{1,0:T(8,128)(2,1)} collective-permute-done((bf16[256,2048]{1,0:T(8,128)(2,1)S(1)}, bf16[256,2048]{1,0:T(8,128)(2,1)}, u32[]{:S(2)}, u32[]{:S(2)}) %collective-permute-start.9) | collective-permute-done | bytes 1048608 | tf_op jit(solution)/shard_map/ppermute | solution.py:498
  93.6 21.4 %collective-permute-done.11.rest_9_ = bf16[256,2048]{1,0:T(8,128)(2,1)} collective-permute-done((bf16[256,2048]{1,0:T(8,128)(2,1)}, bf16[256,2048]{1,0:T(8,128)(2,1)}, u32[]{:S(2)}, u32[]{:S(2)}) %collective-permute-start.11) | collective-permute-done | bytes 1048608 | tf_op jit(solution)/shard_map/ppermute | solution.py:498
  122.8 8.2 %collective-permute-done.13.rest_11_ = bf16[128,2048]{1,0:T(8,128)(2,1)S(1)} collective-permute-done((bf16[128,2048]{1,0:T(8,128)(2,1)S(1)}, bf16[128,2048]{1,0:T(8,128)(2,1)S(1)}, u32[]{:S(2)}, u32[]{:S(2)}) %collective-permute-start.13) | collective-permute-done | bytes 524320 | tf_op jit(solution)/shard_map/ppermute | solution.py:498
  133.3 25.0 %up_project.1 = (bf16[1024,2048]{1,0:T(8,128)(2,1)}, bf16[512,2048]{1,0:T(8,128)(2,1)}, bf16[512,2048]{1,0:T(8,128)(2,1)}) custom-call(s32[9]{0:T(128)} %pad_add_fusion.2.order, bf16[512,2048]{1,0:T(8,128)(2,1)} %collective-permute-done.3.rest_0_, bf16[512,2048]{1,0:T(8,128)(2,1)} %collective-permute-done.5.rest_1_, bf16[512,2048]{1,0:T(8,128)(2,1)} %copy-done.3, ...), custom_call_target="tpu_custom_call" | custom-call | flops 17179869184 | bytes 8388608 | tf_op jit(solution)/shard_map/up_project/pallas_call | solution.py:292
  160.7 2.5 share_of.6
  165.9 2.7 sum_of.6
  168.6 20.2 %collective-permute-done.20.rest_0_ = bf16[2048,256]{1,0:T(8,128)(2,1)S(1)} collective-permute-done((bf16[2048,256]{1,0:T(8,128)(2,1)S(1)}, bf16[2048,256]{1,0:T(8,128)(2,1)S(1)}, u32[]{:S(2)}, u32[]{:S(2)}) %collective-permute-start.20) | collective-permute-done | bytes 1048608 | tf_op jit(solution)/shard_map/ppermute | solution.py:498
  190.1 2.5 share_of.7
  195.4 2.7 sum_of.7
  198.1 20.2 %collective-permute-done.23.rest_0_ = bf16[2048,256]{1,0:T(8,128)(2,1)S(1)} collective-permute-done((bf16[2048,256]{1,0:T(8,128)(2,1)S(1)}, bf16[2048,256]{1,0:T(8,128)(2,1)S(1)}, u32[]{:S(2)}, u32[]{:S(2)}) %collective-permute-start.23) | collective-permute-done | bytes 1048608 | tf_op jit(solution)/shard_map/ppermute | solution.py:498
  219.6 2.5 share_of.8
  226.0 2.7 sum_of.8
  229.5 7.2 %collective-permute-done.26.rest_0_ = bf16[1024,256]{1,0:T(8,128)(2,1)S(1)} collective-permute-done((bf16[1024,256]{1,0:T(8,128)(2,1)S(1)}, bf16[1024,256]{1,0:T(8,128)(2,1)S(1)}, u32[]{:S(2)}, u32[]{:S(2)}) %collective-permute-start.26) | collective-permute-done | bytes 524320 | tf_op jit(solution)/shard_map/ppermute | solution.py:498
  249.7 33.1 %collective-permute-done.29.rest_5_ = bf16[512,256]{1,0:T(8,128)(2,1)} collective-permute-done((bf16[512,256]{1,0:T(8,128)(2,1)}, bf16[512,256]{1,0:T(8,128)(2,1)}, u32[]{:S(2)}, u32[]{:S(2)}) %collective-permute-start.29) | collective-permute-done | bytes 262176 | tf_op jit(solution)/shard_map/ppermute | solution.py:498
  282.9 5.1 %collective-permute-done.33.rest_9_ = bf16[512,256]{1,0:T(8,128)(2,1)} collective-permute-done((bf16[512,256]{1,0:T(8,128)(2,1)}, bf16[512,256]{1,0:T(8,128)(2,1)}, u32[]{:S(2)}, u32[]{:S(2)}) %collective-permute-start.33) | collective-permute-done | bytes 262176 | tf_op jit(solution)/shard_map/ppermute | solution.py:498
  289.9 5.2 %norm_sum.1 = bf16[512,2048]{1,0:T(8,128)(2,1)} custom-call(s32[8]{0:T(128)S(1)} %stack.53.order, bf16[512,2048]{1,0:T(8,128)(2,1)S(1)} %copy-done.4, f32[1,2048]{1,0:T(1,128)S(1)} %bitcast.17, bf16[512,256]{1,0:T(8,128)(2,1)S(1)} %get-tuple-element.29.rest_0_, bf16[512,512]{1,0:T(8,128)(2,1)S(1)} %get-tuple-element.32.rest_1_, ...), custom_call_target="tpu_custom_call" | custom-call | tf_op jit(solution)/shard_map/norm_sum/pallas_call | solution.py:433
  (135 shorter events, 64.5 us)
Async XLA Ops:
  17.9 16.2 %collective-permute-start.6 = (bf16[128,2048]{1,0:T(8,128)(2,1)}, bf16[128,2048]{1,0:T(8,128)(2,1)}, u32[]{:S(2)}, u32[]{:S(2)}) collective-permute-start(bf16[128,2048]{1,0:T(8,128)(2,1)} %constant_dynamic-slice_fusion.1), channel_id=1, source_target_pairs={{0,2},{2,0},{4,6},{6,4},{8,10},{10,8},{12,14},{14,12},{16,18},{18,... | collective-permute-start | bytes 1572872 | tf_op jit(solution)/shard_map/ppermute | solution.py:498
  32.6 46.9 %collective-permute-start.4 = (bf16[512,2048]{1,0:T(8,128)(2,1)S(1)}, bf16[512,2048]{1,0:T(8,128)(2,1)}, u32[]{:S(2)}, u32[]{:S(2)}) collective-permute-start(bf16[512,2048]{1,0:T(8,128)(2,1)S(1)} %multiply_convert_fusion.rest_2_.stream), channel_id=1, source_target_pairs={{0,1},{1,0},{2,3},{3,2},{4,5},{5,4},{6,7},{7,6},{8,9},{9,8},{10,11... | collective-permute-start | bytes 6291464 | tf_op jit(solution)/shard_map/ppermute | solution.py:498
  35.5 29.7 %collective-permute-start.7 = (bf16[256,2048]{1,0:T(8,128)(2,1)S(1)}, bf16[256,2048]{1,0:T(8,128)(2,1)S(1)}, u32[]{:S(2)}, u32[]{:S(2)}) collective-permute-start(bf16[256,2048]{1,0:T(8,128)(2,1)S(1)} %pad_maximum_fusion.1.rest_4_), channel_id=1, source_target_pairs={{0,8},{2,10},{4,0},{6,2},{8,16},{10,18},{12,4},{14,6},{16,24},{18,... | collective-permute-start | bytes 3145736 | tf_op jit(solution)/shard_map/ppermute | solution.py:498
  42.9 24.8 %collective-permute-start.8 = (bf16[256,2048]{1,0:T(8,128)(2,1)S(1)}, bf16[256,2048]{1,0:T(8,128)(2,1)S(1)}, u32[]{:S(2)}, u32[]{:S(2)}) collective-permute-start(bf16[256,2048]{1,0:T(8,128)(2,1)S(1)} %pad_maximum_fusion.1.rest_4_), channel_id=1, source_target_pairs={{0,4},{2,6},{4,12},{6,14},{8,0},{10,2},{12,20},{14,22},{16,8},{18,... | collective-permute-start | bytes 3145736 | tf_op jit(solution)/shard_map/ppermute | solution.py:498
  65.2 24.7 %collective-permute-start.9 = (bf16[256,2048]{1,0:T(8,128)(2,1)S(1)}, bf16[256,2048]{1,0:T(8,128)(2,1)}, u32[]{:S(2)}, u32[]{:S(2)}) collective-permute-start(bf16[256,2048]{1,0:T(8,128)(2,1)S(1)} %collective-permute-done.7.rest_5_), channel_id=1, source_target_pairs={{0,8},{2,10},{4,0},{6,2},{8,16},{10,18},{12,4},{14,6},{16,24},{18,... | collective-permute-start | bytes 3145736 | tf_op jit(solution)/shard_map/ppermute | solution.py:498
  67.7 24.2 %collective-permute-start.10 = (bf16[256,2048]{1,0:T(8,128)(2,1)S(1)}, bf16[256,2048]{1,0:T(8,128)(2,1)}, u32[]{:S(2)}, u32[]{:S(2)}) collective-permute-start(bf16[256,2048]{1,0:T(8,128)(2,1)S(1)} %collective-permute-done.8.rest_6_), channel_id=1, source_target_pairs={{0,4},{2,6},{4,12},{6,14},{8,0},{10,2},{12,20},{14,22},{16,8},{18,... | collective-permute-start | bytes 3145736 | tf_op jit(solution)/shard_map/ppermute | solution.py:498
  67.7 53.4 %collective-permute-start.3 = (bf16[512,2048]{1,0:T(8,128)(2,1)S(1)}, bf16[512,2048]{1,0:T(8,128)(2,1)}, u32[]{:S(2)}, u32[]{:S(2)}) collective-permute-start(bf16[512,2048]{1,0:T(8,128)(2,1)S(1)} %multiply_convert_fusion.rest_2_.stream), channel_id=1, source_target_pairs={{0,2},{2,0},{4,6},{6,4},{8,10},{10,8},{12,14},{14,12},{16,18},{18,... | collective-permute-start | bytes 6291464 | tf_op jit(solution)/shard_map/ppermute | solution.py:498
  79.5 53.8 %collective-permute-start.5 = (bf16[512,2048]{1,0:T(8,128)(2,1)}, bf16[512,2048]{1,0:T(8,128)(2,1)}, u32[]{:S(2)}, u32[]{:S(2)}) collective-permute-start(bf16[512,2048]{1,0:T(8,128)(2,1)} %collective-permute-done.4.rest_3_), channel_id=1, source_target_pairs={{0,2},{2,0},{4,6},{6,4},{8,10},{10,8},{12,14},{14,12},{16,18},{18,... | collective-permute-start | bytes 6291464 | tf_op jit(solution)/shard_map/ppermute | solution.py:498
  90.0 25.0 %collective-permute-start.11 = (bf16[256,2048]{1,0:T(8,128)(2,1)}, bf16[256,2048]{1,0:T(8,128)(2,1)}, u32[]{:S(2)}, u32[]{:S(2)}) collective-permute-start(bf16[256,2048]{1,0:T(8,128)(2,1)} %collective-permute-done.9.rest_7_), channel_id=1, source_target_pairs={{0,8},{2,10},{4,0},{6,2},{8,16},{10,18},{12,4},{14,6},{16,24},{18,... | collective-permute-start | bytes 3145736 | tf_op jit(solution)/shard_map/ppermute | solution.py:498
  91.9 24.7 %collective-permute-start.12 = (bf16[256,2048]{1,0:T(8,128)(2,1)}, bf16[256,2048]{1,0:T(8,128)(2,1)}, u32[]{:S(2)}, u32[]{:S(2)}) collective-permute-start(bf16[256,2048]{1,0:T(8,128)(2,1)} %collective-permute-done.10.rest_8_), channel_id=1, source_target_pairs={{0,4},{2,6},{4,12},{6,14},{8,0},{10,2},{12,20},{14,22},{16,8},{18,... | collective-permute-start | bytes 3145736 | tf_op jit(solution)/shard_map/ppermute | solution.py:498
  92.8 26.5 %collective-permute-start.15 = (bf16[2048,128]{1,0:T(8,128)(2,1)}, bf16[2048,128]{1,0:T(8,128)(2,1)}, u32[]{:S(2)}, u32[]{:S(2)}) collective-permute-start(bf16[2048,128]{1,0:T(8,128)(2,1)} %constant_dynamic-slice_fusion), channel_id=1, source_target_pairs={{0,2},{2,0},{4,6},{6,4},{8,10},{10,8},{12,14},{14,12},{16,18},{18,... | collective-permute-start | bytes 1572872 | tf_op jit(solution)/shard_map/ppermute | solution.py:498
  117.6 14.8 %collective-permute-start.14 = (bf16[128,2048]{1,0:T(8,128)(2,1)S(1)}, bf16[128,2048]{1,0:T(8,128)(2,1)S(1)}, u32[]{:S(2)}, u32[]{:S(2)}) collective-permute-start(bf16[128,2048]{1,0:T(8,128)(2,1)S(1)} %slice.31), channel_id=1, source_target_pairs={{0,4},{2,6},{4,12},{6,14},{8,0},{10,2},{12,20},{14,22},{16,8},{18,... | collective-permute-start | bytes 1572872 | tf_op jit(solution)/shard_map/ppermute | solution.py:498
  120.7 37.6 %collective-permute-start.17 = (bf16[2048,256]{1,0:T(8,128)(2,1)S(1)}, bf16[2048,256]{1,0:T(8,128)(2,1)S(1)}, u32[]{:S(2)}, u32[]{:S(2)}) collective-permute-start(bf16[2048,256]{1,0:T(8,128)(2,1)S(1)} %pad_maximum_fusion.2.rest_0_), channel_id=1, source_target_pairs={{0,8},{2,10},{4,0},{6,2},{8,16},{10,18},{12,4},{14,6},{16,24},{18,... | collective-permute-start | bytes 3145736 | tf_op jit(solution)/shard_map/ppermute | solution.py:498
  121.2 37.2 %collective-permute-start.18 = (bf16[2048,256]{1,0:T(8,128)(2,1)S(1)}, bf16[2048,256]{1,0:T(8,128)(2,1)S(1)}, u32[]{:S(2)}, u32[]{:S(2)}) collective-permute-start(bf16[2048,256]{1,0:T(8,128)(2,1)S(1)} %pad_maximum_fusion.2.rest_0_), channel_id=1, source_target_pairs={{0,4},{2,6},{4,12},{6,14},{8,0},{10,2},{12,20},{14,22},{16,8},{18,... | collective-permute-start | bytes 3145736 | tf_op jit(solution)/shard_map/ppermute | solution.py:498
  163.3 25.6 %collective-permute-start.20 = (bf16[2048,256]{1,0:T(8,128)(2,1)S(1)}, bf16[2048,256]{1,0:T(8,128)(2,1)S(1)}, u32[]{:S(2)}, u32[]{:S(2)}) collective-permute-start(bf16[2048,256]{1,0:T(8,128)(2,1)S(1)} %collective-permute-done.17.rest_0_), channel_id=1, source_target_pairs={{0,8},{2,10},{4,0},{6,2},{8,16},{10,18},{12,4},{14,6},{16,24},{18,... | collective-permute-start | bytes 3145736 | tf_op jit(solution)/shard_map/ppermute | solution.py:498
  164.9 25.2 %collective-permute-start.21 = (bf16[2048,256]{1,0:T(8,128)(2,1)S(1)}, bf16[2048,256]{1,0:T(8,128)(2,1)S(1)}, u32[]{:S(2)}, u32[]{:S(2)}) collective-permute-start(bf16[2048,256]{1,0:T(8,128)(2,1)S(1)} %collective-permute-done.18.rest_1_), channel_id=1, source_target_pairs={{0,4},{2,6},{4,12},{6,14},{8,0},{10,2},{12,20},{14,22},{16,8},{18,... | collective-permute-start | bytes 3145736 | tf_op jit(solution)/shard_map/ppermute | solution.py:498
  192.8 25.6 %collective-permute-start.23 = (bf16[2048,256]{1,0:T(8,128)(2,1)S(1)}, bf16[2048,256]{1,0:T(8,128)(2,1)S(1)}, u32[]{:S(2)}, u32[]{:S(2)}) collective-permute-start(bf16[2048,256]{1,0:T(8,128)(2,1)S(1)} %collective-permute-done.20.rest_0_), channel_id=1, source_target_pairs={{0,8},{2,10},{4,0},{6,2},{8,16},{10,18},{12,4},{14,6},{16,24},{18,... | collective-permute-start | bytes 3145736 | tf_op jit(solution)/shard_map/ppermute | solution.py:498
  194.4 25.2 %collective-permute-start.24 = (bf16[2048,256]{1,0:T(8,128)(2,1)S(1)}, bf16[2048,256]{1,0:T(8,128)(2,1)S(1)}, u32[]{:S(2)}, u32[]{:S(2)}) collective-permute-start(bf16[2048,256]{1,0:T(8,128)(2,1)S(1)} %collective-permute-done.21.rest_1_), channel_id=1, source_target_pairs={{0,4},{2,6},{4,12},{6,14},{8,0},{10,2},{12,20},{14,22},{16,8},{18,... | collective-permute-start | bytes 3145736 | tf_op jit(solution)/shard_map/ppermute | solution.py:498
  225.9 16.9 %collective-permute-start.16 = (bf16[1024,256]{1,0:T(8,128)(2,1)S(1)}, bf16[1024,256]{1,0:T(8,128)(2,1)S(1)}, u32[]{:S(2)}, u32[]{:S(2)}) collective-permute-start(bf16[1024,256]{1,0:T(8,128)(2,1)S(1)} %share_of.5), channel_id=1, source_target_pairs={{0,2},{2,0},{4,6},{6,4},{8,10},{10,8},{12,14},{14,12},{16,18},{18,... | collective-permute-start | bytes 1572872 | tf_op jit(solution)/shard_map/ppermute | solution.py:498
  239.6 43.3 %collective-permute-start.30 = (bf16[512,512]{1,0:T(8,128)(2,1)}, bf16[512,512]{1,0:T(8,128)(2,1)}, u32[]{:S(2)}, u32[]{:S(2)}) collective-permute-start(bf16[512,512]{1,0:T(8,128)(2,1)} %get-tuple-element.33), channel_id=1, source_target_pairs={{0,1},{1,0},{2,3},{3,2},{4,5},{5,4},{6,7},{7,6},{8,9},{9,8},{10,11... | collective-permute-start | bytes 1572872 | tf_op jit(solution)/shard_map/ppermute | solution.py:498
  240.7 42.1 %collective-permute-start.31 = (bf16[512,512]{1,0:T(8,128)(2,1)}, bf16[512,512]{1,0:T(8,128)(2,1)}, u32[]{:S(2)}, u32[]{:S(2)}) collective-permute-start(bf16[512,512]{1,0:T(8,128)(2,1)} %get-tuple-element.37), channel_id=1, source_target_pairs={{0,1},{1,0},{2,3},{3,2},{4,5},{5,4},{6,7},{7,6},{8,9},{9,8},{10,11... | collective-permute-start | bytes 1572872 | tf_op jit(solution)/shard_map/ppermute | solution.py:498
  241.7 41.2 %collective-permute-start.32 = (bf16[512,512]{1,0:T(8,128)(2,1)}, bf16[512,512]{1,0:T(8,128)(2,1)}, u32[]{:S(2)}, u32[]{:S(2)}) collective-permute-start(bf16[512,512]{1,0:T(8,128)(2,1)} %get-tuple-element.41), channel_id=1, source_target_pairs={{0,1},{1,0},{2,3},{3,2},{4,5},{5,4},{6,7},{7,6},{8,9},{9,8},{10,11... | collective-permute-start | bytes 1572872 | tf_op jit(solution)/shard_map/ppermute | solution.py:498
  244.8 38.0 %collective-permute-start.29 = (bf16[512,256]{1,0:T(8,128)(2,1)}, bf16[512,256]{1,0:T(8,128)(2,1)}, u32[]{:S(2)}, u32[]{:S(2)}) collective-permute-start(bf16[512,256]{1,0:T(8,128)(2,1)} %get-tuple-element.45), channel_id=1, source_target_pairs={{0,1},{1,0},{2,3},{3,2},{4,5},{5,4},{6,7},{7,6},{8,9},{9,8},{10,11... | collective-permute-start | bytes 786440 | tf_op jit(solution)/shard_map/ppermute | solution.py:498
  248.6 39.3 %collective-permute-start.33 = (bf16[512,256]{1,0:T(8,128)(2,1)}, bf16[512,256]{1,0:T(8,128)(2,1)}, u32[]{:S(2)}, u32[]{:S(2)}) collective-permute-start(bf16[512,256]{1,0:T(8,128)(2,1)} %get-tuple-element.46), channel_id=1, source_target_pairs={{0,1},{1,0},{2,3},{3,2},{4,5},{5,4},{6,7},{7,6},{8,9},{9,8},{10,11... | collective-permute-start | bytes 786440 | tf_op jit(solution)/shard_map/ppermute | solution.py:498
  (35 other events, 474.2 us)

commit v3 on v2

--- a/solution.py
+++ b/solution.py
@@ -241,32 +241,32 @@
     return len(zs), len(ys), len(cores)
 
 
-def up_body(tile, unit, order, *rest):
-    count = order.shape[0]
-    rows = rest[:4]
-    weights = rest[4 : 4 + count]
-    outs = rest[4 + count : 7 + count]
-    buffer, sems = rest[7 + count :]
+def up_body(tile, order, *rest):
+    count = len(rest) - 7
+    rows = rest[:2]
+    weights = rest[2 : 2 + count]
+    out, picked, buffer, row_sems, sems = rest[2 + count :]
     step = pl.program_id(0)
     steps = pl.num_programs(0)
+    unit = weights[0].shape[0]
+    size = rows[0].shape[0]
 
     def copies(index, slot):
         return [
             pltpu.make_async_copy(
                 weight.at[:, pl.ds(pl.multiple_of(index * tile, tile), tile)],
-                buffer.at[
-                    slot, pl.ds(pl.multiple_of(order[j] * unit, unit), weight.shape[0]), :
-                ],
+                buffer.at[slot, j * unit : (j + 1) * unit, :],
                 sems.at[slot, j],
             )
             for j, weight in enumerate(weights)
         ]
 
+    row_copies = pick_copies(order, 0, rows, count, picked, row_sems)
     slot = lax.rem(step, 2)
 
     @pl.when(step == 0)
     def _():
-        for copy in copies(step, slot):
+        for copy in (*row_copies, *copies(step, slot)):
             copy.start()
 
     @pl.when(step + 1 < steps)
@@ -274,48 +274,137 @@
         for copy in copies(step + 1, 1 - slot):
             copy.start()
 
+    @pl.when(step == 0)
+    def _():
+        for copy in row_copies:
+            copy.wait()
+
     for copy in copies(step, slot):
         copy.wait()
-    size = rows[0].shape[0]
-    places = ((outs[0], 0), (outs[0], size), (outs[1], 0), (outs[2], 0))
-    for part, (out, first) in zip(rows, places):
-        hidden = jnp.dot(part[...], buffer[slot], preferred_element_type=jnp.float32)
-        out[first : first + size] = jnp.square(jnp.maximum(hidden, 0.0)).astype(out.dtype)
-
-
-def up_project(order, rows, weights):
+    for number in range(2):
+        at = slice(number * size, (number + 1) * size)
+        out[at] = jnp.dot(picked[at], buffer[slot], preferred_element_type=jnp.float32)
+
+
+def pick_copies(order, first, rows, count, picked, sems):
+    size, width = rows[0].shape
+    unit = width // order.shape[0]
+    return [
+        pltpu.make_async_copy(
+            part.at[:, pl.ds(pl.multiple_of(order[first + j] * unit, unit), unit)],
+            picked.at[number * size : (number + 1) * size, j * unit : (j + 1) * unit],
+            sems.at[number, j],
+        )
+        for number, part in enumerate(rows)
+        for j in range(count)
+    ]
+
+
+def up_partial(order, rows, weights):
     hidden_units = weights[0].shape[1]
-    unit = min(weight.shape[0] for weight in weights)
+    unit = weights[0].shape[0]
     tile = min(512, hidden_units)
-    count, width = rows[0].shape
-    dtype = rows[0].dtype
+    count = rows[0].shape[0]
+    depth = unit * len(weights)
     return pl.pallas_call(
-        functools.partial(up_body, tile, unit),
+        functools.partial(up_body, tile),
         grid_spec=pltpu.PrefetchScalarGridSpec(
             num_scalar_prefetch=1,
             grid=(hidden_units // tile,),
-            in_specs=[pl.BlockSpec((count, width), lambda n, order: (0, 0))] * 4
-            + [pl.BlockSpec(memory_space=pl.ANY)] * len(weights),
+            in_specs=[pl.BlockSpec(memory_space=pl.ANY)] * (2 + len(weights)),
+            out_specs=pl.BlockSpec((2 * count, tile), lambda n, order: (0, n)),
+            scratch_shapes=[
+                pltpu.VMEM((2 * count, depth), rows[0].dtype),
+                pltpu.VMEM((2, depth, tile), rows[0].dtype),
+                pltpu.SemaphoreType.DMA((2, len(weights))),
+                pltpu.SemaphoreType.DMA((2, len(weights))),
+            ],
+        ),
+        out_shape=jax.ShapeDtypeStruct((2 * count, hidden_units), jnp.float32),
+        cost_estimate=pl.CostEstimate(
+            flops=4 * count * depth * hidden_units,
+            bytes_accessed=2 * depth * hidden_units,
+            transcendentals=0,
+        ),
+        compiler_params=pltpu.CompilerParams(vmem_limit_bytes=VMEM_LARGE),
+        name="up_partial",
+    )(order, *rows, *weights)
+
+
+def finish_body(first, order, *rest):
+    rows = rest[:4]
+    near, far = rest[4:6]
+    weights = rest[6:-6]
+    outs = rest[-6:-3]
+    picked, joined, row_sems = rest[-3:]
+    unit = rows[0].shape[1] // order.shape[0]
+    row_copies = pick_copies(order, first, rows, picked.shape[1] // unit, picked, row_sems)
+
+    @pl.when(pl.program_id(0) == 0)
+    def _():
+        for copy in row_copies:
+            copy.start()
+
+    at = 0
+    for weight in weights:
+        joined[at : at + weight.shape[0]] = weight[...]
+        at += weight.shape[0]
+
+    @pl.when(pl.program_id(0) == 0)
+    def _():
+        for copy in row_copies:
+            copy.wait()
+
+    size = rows[0].shape[0]
+    one, two = slice(0, size), slice(size, 2 * size)
+    places = ((near, one, outs[0], one), (far, one, outs[0], two))
+    places += ((near, two, outs[1], one), (far, two, outs[2], one))
+    for number, (partial, source, out, target) in enumerate(places):
+        hidden = partial[source] + jnp.dot(
+            picked[number * size : (number + 1) * size],
+            joined[...],
+            preferred_element_type=jnp.float32,
+        )
+        out[target] = jnp.square(jnp.maximum(hidden, 0.0)).astype(out.dtype)
+
+
+def up_finish(order, first, rows, near, far, weights):
+    count, width = rows[0].shape
+    hidden_units = near.shape[1]
+    tile = min(512, hidden_units)
+    dtype = rows[0].dtype
+    depth = sum(weight.shape[0] for weight in weights)
+    return pl.pallas_call(
+        functools.partial(finish_body, first),
+        grid_spec=pltpu.PrefetchScalarGridSpec(
+            num_scalar_prefetch=1,
+            grid=(hidden_units // tile,),
+            in_specs=[
+                *[pl.BlockSpec(memory_space=pl.ANY)] * 4,
+                *[pl.BlockSpec((2 * count, tile), lambda n, order: (0, n))] * 2,
+                *[pl.BlockSpec((w.shape[0], tile), lambda n, order: (0, n)) for w in weights],
+            ],
             out_specs=[
                 pl.BlockSpec((size, tile), lambda n, order: (0, n))
                 for size in (2 * count, count, count)
             ],
             scratch_shapes=[
-                pltpu.VMEM((2, width, tile), dtype),
-                pltpu.SemaphoreType.DMA((2, len(weights))),
+                pltpu.VMEM((4 * count, depth), dtype),
+                pltpu.VMEM((depth, tile), dtype),
+                pltpu.SemaphoreType.DMA((4, depth * order.shape[0] // width)),
             ],
         ),
         out_shape=[
             jax.ShapeDtypeStruct((size, hidden_units), dtype) for size in (2 * count, count, count)
         ],
         cost_estimate=pl.CostEstimate(
-            flops=8 * count * width * hidden_units,
-            bytes_accessed=2 * width * hidden_units,
+            flops=8 * count * depth * hidden_units,
+            bytes_accessed=24 * count * hidden_units,
             transcendentals=0,
         ),
         compiler_params=pltpu.CompilerParams(vmem_limit_bytes=VMEM_LARGE),
-        name="up_project",
-    )(order, *rows, *weights)
+        name="up_finish",
+    )(order, *rows, near, far, *weights)
 
 
 def block_dots(rows, weights):
@@ -519,7 +608,9 @@
     for _ in range(1, chips // 2):
         left, right = pass_on(left, right)
         up_blocks += [left, right]
-    up_blocks += pass_on(half(left, 0), half(right, 1))
+    early = 2 * (chips // 2 - 2) + 1
+    up_late = up_blocks[early:]
+    up_last = (left, right)
     down_own = halved(down_weight, 0)
 
     place = jnp.where(my_y == 0, my_z, chips - 1 - my_z)
@@ -532,8 +623,6 @@
     for step in range(1, chips // 2):
         steps += [-step, step]
     order = jnp.stack([chip_at(by) for by in (*steps, chips // 2)]).astype(jnp.int32)
-    last = 2 * order[-1:]
-    up_order = jnp.concatenate([2 * order[:-1], last, last + 1])
 
     kv_heads = keyvals.shape[1]
     tok_rows = queries.shape[0]
@@ -569,15 +658,24 @@
     peer_stream = send(first_stream, swap, "tp")
     twin_stream = send(first_stream, twin)
     far_stream = send(peer_stream, twin)
-    twin_active, own_active, peer_active = up_project(
-        up_order, (twin_stream, far_stream, first_stream, peer_stream), up_blocks
-    )
 
     def after(value, *results):
         return lax.optimization_barrier((value, *results))[0]
 
+    near = up_partial(order, (twin_stream, first_stream), up_blocks[:early])
+    left, right = (after(block, near) for block in up_last)
+    up_late += pass_on(half(left, 0), half(right, 1))
+    far = up_partial(order, (far_stream, peer_stream), up_blocks[:early])
+    twin_active, own_active, peer_active = up_finish(
+        order,
+        early,
+        (twin_stream, far_stream, first_stream, peer_stream),
+        near,
+        far,
+        up_late,
+    )
+
     left, right = pass_on(down_own, down_own)
-    left, right = after(left, twin_active), after(right, twin_active)
     mine, theirs = [], []
 
     def share(weights):
@@ -601,7 +699,8 @@
         if step == 1:
             summed(from_twin, (down_own,))
         done = summed(from_twin_too, pair)
-        left, right = after(left, done), after(right, done)
+        if step > 1:
+            left, right = after(left, done), after(right, done)
     return norm_sum(order, first_stream, second_gain, mine, theirs)
 
 

time: 296 us -> 280 us (0.946)
  waiting for transfers between devices: 168 us -> 146 us
  Pallas kernels: 63 us -> 75.6 us
  local copies, waits for them, and re-layouts: 12.6 us -> 8.87 us
    ppermute x34, waiting for transfers between devices: 168 us -> 146 us  [send(): return lax.ppermute(value, axis, way)]
    pallas_call x1 -> x3, Pallas kernels: 25 us -> 38.5 us  [the longest x2 22.7 us: up_partial(): pl.pallas_call(functools.partial(up_body, tile), grid_spec=pltpu.Prefetch...]
    unnamed x51 -> x45, local copies, waits for them, and re-layouts: 8.3 us -> 5.14 us
  transfers between devices with their start and end apart: 34 -> 34, of which waited for: 18 -> 16; matrix products, arithmetic and copies ran while one was open for 5% -> 4% of each run, Pallas kernels for 15% -> 22%
where the time goes in v3:
time: 280 us; the launch traced here: 279 us
  waiting for transfers between devices  146 us (52%)
  Pallas kernels  75.6 us (27%)
  starting transfers between devices  40.5 us (14%)
  local copies, waits for them, and re-layouts  8.87 us (3%)
  other arithmetic  5.52 us (2%)
    ppermute x34, waiting for transfers between devices, send(): return lax.ppermute(value, axis, way)  146 us
    ppermute x34, starting transfers between devices, send(): return lax.ppermute(value, axis, way)  40.5 us
    pallas_call x2, Pallas kernels, up_partial(): pl.pallas_call(functools.partial(up_body, tile), grid_spec=pltpu.Prefetch...  22.7 us
    pallas_call x1, Pallas kernels, up_finish(): pl.pallas_call(functools.partial(finish_body, first), grid_spec=pltpu.Pre...  15.8 us
    pallas_call x5, Pallas kernels, share_of(): pl.pallas_call(functools.partial(share_body, len(weights)), grid=(count /...  11.7 us
    pallas_call x5, Pallas kernels, sum_of(): pl.pallas_call(functools.partial(sum_body, len(weights)), grid=(steps,),...  11.7 us
    pallas_call x2, Pallas kernels, attend_rows(): pl.pallas_call(functools.partial(attend_body, kv_heads, total_rows), grid...  10.2 us
  transfers between devices with their start and end apart: 34, of which 16 were waited for; matrix products, arithmetic and copies ran while one was open for 4% of the time, Pallas kernels for 22%

profile of v3, /device:TPU:0, one launch (start us, length us, event | category | flops | bytes accessed | tf_op | source)
XLA Modules:
  0.0 279.1 jit_solution(6627355824459240506)
XLA Ops:
  1.7 2.5 collective-permute-start
  7.0 2.7 collective-permute-done.1.high
  9.7 5.1 %attend_rows.3 = bf16[512,512]{1,0:T(8,128)(2,1)S(1)} custom-call(s32[2]{0:T(128)S(1)} %pad_add_fusion.1.place, f32[8]{0:T(128)S(1)} %copy-done.8, bf16[1024,512]{1,0:T(8,128)(2,1)S(1)} %copy-done.7, bf16[128,640]{1,0:T(8,128)(2,1)S(1)} %collective-permute-done.low, bf16[1024,640]{1,0:T(8,128)(2,1)S(1)} %pad_maximum_fusion.own, ...), custom_call_target="tpu_custom_call" | custom-call | flops 4026531840 | bytes 2097152 | tf_op jit(solution)/shard_map/attend_rows/pallas_call | solution.py:201
  17.2 3.6 %collective-permute-start.6 = (bf16[128,2048]{1,0:T(8,128)(2,1)}, bf16[128,2048]{1,0:T(8,128)(2,1)}, u32[]{:S(2)}, u32[]{:S(2)}) collective-permute-start(bf16[128,2048]{1,0:T(8,128)(2,1)} %constant_dynamic-slice_fusion.1), channel_id=1, source_target_pairs={{0,2},{2,0},{4,6},{6,4},{8,10},{10,8},{12,14},{14,12},{16,18},{18,... | collective-permute-start | bytes 1572872 | tf_op jit(solution)/shard_map/ppermute | solution.py:587
  20.9 5.1 %attend_rows.2 = bf16[512,512]{1,0:T(8,128)(2,1)S(1)} custom-call(s32[2]{0:T(128)S(1)} %pad_add_fusion.place, f32[8]{0:T(128)S(1)} %copy-done.8, bf16[1024,512]{1,0:T(8,128)(2,1)S(1)} %copy-done.7, bf16[128,640]{1,0:T(8,128)(2,1)S(1)} %collective-permute-done.low, bf16[1024,640]{1,0:T(8,128)(2,1)S(1)} %pad_maximum_fusion.own, ...), custom_call_target="tpu_custom_call" | custom-call | flops 4026531840 | bytes 2097152 | tf_op jit(solution)/shard_map/attend_rows/pallas_call | solution.py:201
  34.9 4.8 %collective-permute-start.8 = (bf16[256,2048]{1,0:T(8,128)(2,1)S(1)}, bf16[256,2048]{1,0:T(8,128)(2,1)S(1)}, u32[]{:S(2)}, u32[]{:S(2)}) collective-permute-start(bf16[256,2048]{1,0:T(8,128)(2,1)S(1)} %pad_maximum_fusion.1.rest_2_), channel_id=1, source_target_pairs={{0,4},{2,6},{4,12},{6,14},{8,0},{10,2},{12,20},{14,22},{16,8},{18,... | collective-permute-start | bytes 3145736 | tf_op jit(solution)/shard_map/ppermute | solution.py:587
  39.6 2.7 collective-permute-start.7
  42.3 23.0 %collective-permute-done.8.rest_4_ = bf16[256,2048]{1,0:T(8,128)(2,1)S(1)} collective-permute-done((bf16[256,2048]{1,0:T(8,128)(2,1)S(1)}, bf16[256,2048]{1,0:T(8,128)(2,1)S(1)}, u32[]{:S(2)}, u32[]{:S(2)}) %collective-permute-start.8) | collective-permute-done | bytes 1048608 | tf_op jit(solution)/shard_map/ppermute | solution.py:587
  67.5 11.4 %collective-permute-done.4.rest_1_.rest_3_ = bf16[512,2048]{1,0:T(8,128)(2,1)} collective-permute-done((bf16[512,2048]{1,0:T(8,128)(2,1)S(1)}, bf16[512,2048]{1,0:T(8,128)(2,1)}, u32[]{:S(2)}, u32[]{:S(2)}) %collective-permute-start.4) | collective-permute-done | bytes 2097184 | tf_op jit(solution)/shard_map/ppermute | solution.py:587
  80.9 10.2 %collective-permute-done.9.rest_5_ = bf16[256,2048]{1,0:T(8,128)(2,1)} collective-permute-done((bf16[256,2048]{1,0:T(8,128)(2,1)S(1)}, bf16[256,2048]{1,0:T(8,128)(2,1)}, u32[]{:S(2)}, u32[]{:S(2)}) %collective-permute-start.9) | collective-permute-done | bytes 1048608 | tf_op jit(solution)/shard_map/ppermute | solution.py:587
  97.2 11.4 %up_partial.2.rest_4_ = f32[1024,2048]{1,0:T(8,128)} custom-call(s32[8]{0:T(128)} %stack.51.order, bf16[512,2048]{1,0:T(8,128)(2,1)} %copy-done.11, bf16[512,2048]{1,0:T(8,128)(2,1)} %copy-done.2, bf16[256,2048]{1,0:T(8,128)(2,1)} %copy-done.12, bf16[256,2048]{1,0:T(8,128)(2,1)} %copy-done.21, bf16[256,2048]{1,0:T(8,128)(2,1)} %copy-done.20, ...), custom_call_target="tpu_custom_call" | custom-call | flops 5368709120 | bytes 5242880 | tf_op jit(solution)/shard_map/up_partial/pallas_call | solution.py:309
  108.6 8.7 %collective-permute-done.11.rest_6_ = bf16[256,2048]{1,0:T(8,128)(2,1)S(1)} collective-permute-done((bf16[256,2048]{1,0:T(8,128)(2,1)}, bf16[256,2048]{1,0:T(8,128)(2,1)S(1)}, u32[]{:S(2)}, u32[]{:S(2)}) %collective-permute-start.11) | collective-permute-done | bytes 1048608 | tf_op jit(solution)/shard_map/ppermute | solution.py:587
  121.3 18.5 %collective-permute-done.17.rest_0_ = bf16[2048,256]{1,0:T(8,128)(2,1)} collective-permute-done((bf16[2048,256]{1,0:T(8,128)(2,1)S(1)}, bf16[2048,256]{1,0:T(8,128)(2,1)}, u32[]{:S(2)}, u32[]{:S(2)}) %collective-permute-start.17) | collective-permute-done | bytes 1048608 | tf_op jit(solution)/shard_map/ppermute | solution.py:587
  141.9 11.4 %up_partial.3.rest_5_ = f32[1024,2048]{1,0:T(8,128)} custom-call(s32[8]{0:T(128)} %stack.51.order, bf16[512,2048]{1,0:T(8,128)(2,1)} %collective-permute-done.5.rest_0_.rest_1_, bf16[512,2048]{1,0:T(8,128)(2,1)} %collective-permute-done.4.rest_1_.rest_3_, bf16[256,2048]{1,0:T(8,128)(2,1)} %copy-done.12, bf16[256,2048]{1,0:T(8,128)(2,1)} %copy-done.21, ...), custom_call_target="tpu_custom_call" | custom-call | flops 5368709120 | bytes 5242880 | tf_op jit(solution)/shard_map/up_partial/pallas_call | solution.py:309
  153.3 15.8 %up_finish.1 = (bf16[1024,2048]{1,0:T(8,128)(2,1)}, bf16[512,2048]{1,0:T(8,128)(2,1)}, bf16[512,2048]{1,0:T(8,128)(2,1)}) custom-call(s32[8]{0:T(128)} %stack.51.order, bf16[512,2048]{1,0:T(8,128)(2,1)} %copy-done.11, bf16[512,2048]{1,0:T(8,128)(2,1)} %collective-permute-done.5.rest_0_.rest_1_, bf16[512,2048]{1,0:T(8,128)(2,1)} %copy-done.2, ...), custom_call_target="tpu_custom_call" | custom-call | flops 6442450944 | bytes 25165824 | tf_op jit(solution)/shard_map/up_finish/pallas_call | solution.py:377
  169.1 2.8 %collective-permute-done.20.rest_0_ = bf16[2048,256]{1,0:T(8,128)(2,1)S(1)} collective-permute-done((bf16[2048,256]{1,0:T(8,128)(2,1)}, bf16[2048,256]{1,0:T(8,128)(2,1)S(1)}, u32[]{:S(2)}, u32[]{:S(2)}) %collective-permute-start.20) | collective-permute-done | bytes 1048608 | tf_op jit(solution)/shard_map/ppermute | solution.py:587
  181.9 20.4 %collective-permute-done.24.rest_1_ = bf16[2048,256]{1,0:T(8,128)(2,1)S(1)} collective-permute-done((bf16[2048,256]{1,0:T(8,128)(2,1)S(1)}, bf16[2048,256]{1,0:T(8,128)(2,1)S(1)}, u32[]{:S(2)}, u32[]{:S(2)}) %collective-permute-start.24) | collective-permute-done | bytes 1048608 | tf_op jit(solution)/shard_map/ppermute | solution.py:587
  206.3 3.8 %share_of.6 = bf16[1024,512]{1,0:T(8,128)(2,1)S(1)} custom-call(bf16[1024,2048]{1,0:T(8,128)(2,1)S(1)} %copy-done.4, bf16[2048,256]{1,0:T(8,128)(2,1)} %collective-permute-done.17.rest_0_, bf16[2048,256]{1,0:T(8,128)(2,1)S(1)} %collective-permute-done.18.rest_1_), custom_call_target="tpu_custom_call" | custom-call | flops 2147483648 | bytes 6291456 | tf_op jit(solution)/shard_map/share_of/pallas_call | solution.py:451
  214.4 2.5 sum_of.8
  216.9 7.7 %collective-permute-done.27.rest_1_ = bf16[1024,256]{1,0:T(8,128)(2,1)S(1)} collective-permute-done((bf16[1024,256]{1,0:T(8,128)(2,1)S(1)}, bf16[1024,256]{1,0:T(8,128)(2,1)S(1)}, u32[]{:S(2)}, u32[]{:S(2)}) %collective-permute-start.27) | collective-permute-done | bytes 524320 | tf_op jit(solution)/shard_map/ppermute | solution.py:587
  228.8 3.7 %sum_of.6 = (bf16[512,512]{1,0:T(8,128)(2,1)S(1)}, bf16[512,512]{1,0:T(8,128)(2,1)S(1)}) custom-call(bf16[512,2048]{1,0:T(8,128)(2,1)S(1)} %copy-done.1, bf16[512,2048]{1,0:T(8,128)(2,1)S(1)} %copy-done, bf16[1024,512]{1,0:T(8,128)(2,1)S(1)} %collective-permute-done.19.from_peer.from_own, bf16[1024,512]{1,0:T(8,128)(2,1)S(1)} %collective-permute-done.19.from_peer.from_own, ...), custom_call_target="tpu_custom_call" | custom-call | flops 2147483648 | bytes 6291456 | tf_op jit(solution)/shard_map/sum_of/pallas_call | solution.py:477
  239.8 30.7 %collective-permute-done.29.rest_5_ = bf16[512,256]{1,0:T(8,128)(2,1)S(1)} collective-permute-done((bf16[512,256]{1,0:T(8,128)(2,1)S(1)}, bf16[512,256]{1,0:T(8,128)(2,1)S(1)}, u32[]{:S(2)}, u32[]{:S(2)}) %collective-permute-start.29) | collective-permute-done | bytes 262176 | tf_op jit(solution)/shard_map/ppermute | solution.py:587
  270.5 5.1 %collective-permute-done.33.rest_9_ = bf16[512,256]{1,0:T(8,128)(2,1)S(1)} collective-permute-done((bf16[512,256]{1,0:T(8,128)(2,1)S(1)}, bf16[512,256]{1,0:T(8,128)(2,1)S(1)}, u32[]{:S(2)}, u32[]{:S(2)}) %collective-permute-start.33) | collective-permute-done | bytes 262176 | tf_op jit(solution)/shard_map/ppermute | solution.py:587
  275.5 3.5 %norm_sum.1 = bf16[512,2048]{1,0:T(8,128)(2,1)} custom-call(s32[8]{0:T(128)S(1)} %copy-done.6, bf16[512,2048]{1,0:T(8,128)(2,1)S(1)} %copy-done.3, f32[1,2048]{1,0:T(1,128)S(1)} %bitcast.17, bf16[512,256]{1,0:T(8,128)(2,1)S(1)} %get-tuple-element.29.rest_0_, bf16[512,512]{1,0:T(8,128)(2,1)S(1)} %get-tuple-element.30.rest_1_, ...), custom_call_target="tpu_custom_call" | custom-call | tf_op jit(solution)/shard_map/norm_sum/pallas_call | solution.py:522
  (128 shorter events, 61.7 us)
Async XLA Ops:
  31.9 46.9 %collective-permute-start.4 = (bf16[512,2048]{1,0:T(8,128)(2,1)S(1)}, bf16[512,2048]{1,0:T(8,128)(2,1)}, u32[]{:S(2)}, u32[]{:S(2)}) collective-permute-start(bf16[512,2048]{1,0:T(8,128)(2,1)S(1)} %multiply_convert_fusion.rest_1_.rest_2_.stream), channel_id=1, source_target_pairs={{0,1},{1,0},{2,3},{3,2},{4,5},{5,4},{6,7},{7,6},{8,9},{9,8},{10,11... | collective-permute-start | bytes 6291464 | tf_op jit(solution)/shard_map/ppermute | solution.py:587
  34.9 30.5 %collective-permute-start.8 = (bf16[256,2048]{1,0:T(8,128)(2,1)S(1)}, bf16[256,2048]{1,0:T(8,128)(2,1)S(1)}, u32[]{:S(2)}, u32[]{:S(2)}) collective-permute-start(bf16[256,2048]{1,0:T(8,128)(2,1)S(1)} %pad_maximum_fusion.1.rest_2_), channel_id=1, source_target_pairs={{0,4},{2,6},{4,12},{6,14},{8,0},{10,2},{12,20},{14,22},{16,8},{18,... | collective-permute-start | bytes 3145736 | tf_op jit(solution)/shard_map/ppermute | solution.py:587
  39.6 26.0 %collective-permute-start.7 = (bf16[256,2048]{1,0:T(8,128)(2,1)S(1)}, bf16[256,2048]{1,0:T(8,128)(2,1)S(1)}, u32[]{:S(2)}, u32[]{:S(2)}) collective-permute-start(bf16[256,2048]{1,0:T(8,128)(2,1)S(1)} %pad_maximum_fusion.1.rest_2_), channel_id=1, source_target_pairs={{0,8},{2,10},{4,0},{6,2},{8,16},{10,18},{12,4},{14,6},{16,24},{18,... | collective-permute-start | bytes 3145736 | tf_op jit(solution)/shard_map/ppermute | solution.py:587
  42.3 51.5 %collective-permute-start.3 = (bf16[512,2048]{1,0:T(8,128)(2,1)S(1)}, bf16[512,2048]{1,0:T(8,128)(2,1)S(1)}, u32[]{:S(2)}, u32[]{:S(2)}) collective-permute-start(bf16[512,2048]{1,0:T(8,128)(2,1)S(1)} %multiply_convert_fusion.rest_1_.rest_2_.stream), channel_id=1, source_target_pairs={{0,2},{2,0},{4,6},{6,4},{8,10},{10,8},{12,14},{14,12},{16,18},{18,... | collective-permute-start | bytes 6291464 | tf_op jit(solution)/shard_map/ppermute | solution.py:587
  65.3 26.2 %collective-permute-start.10 = (bf16[256,2048]{1,0:T(8,128)(2,1)S(1)}, bf16[256,2048]{1,0:T(8,128)(2,1)}, u32[]{:S(2)}, u32[]{:S(2)}) collective-permute-start(bf16[256,2048]{1,0:T(8,128)(2,1)S(1)} %collective-permute-done.8.rest_4_), channel_id=1, source_target_pairs={{0,4},{2,6},{4,12},{6,14},{8,0},{10,2},{12,20},{14,22},{16,8},{18,... | collective-permute-start | bytes 3145736 | tf_op jit(solution)/shard_map/ppermute | solution.py:587
  65.6 25.4 %collective-permute-start.9 = (bf16[256,2048]{1,0:T(8,128)(2,1)S(1)}, bf16[256,2048]{1,0:T(8,128)(2,1)}, u32[]{:S(2)}, u32[]{:S(2)}) collective-permute-start(bf16[256,2048]{1,0:T(8,128)(2,1)S(1)} %collective-permute-done.7.rest_3_), channel_id=1, source_target_pairs={{0,8},{2,10},{4,0},{6,2},{8,16},{10,18},{12,4},{14,6},{16,24},{18,... | collective-permute-start | bytes 3145736 | tf_op jit(solution)/shard_map/ppermute | solution.py:587
  78.8 63.1 %collective-permute-start.5 = (bf16[512,2048]{1,0:T(8,128)(2,1)}, bf16[512,2048]{1,0:T(8,128)(2,1)}, u32[]{:S(2)}, u32[]{:S(2)}) collective-permute-start(bf16[512,2048]{1,0:T(8,128)(2,1)} %collective-permute-done.4.rest_1_.rest_3_), channel_id=1, source_target_pairs={{0,2},{2,0},{4,6},{6,4},{8,10},{10,8},{12,14},{14,12},{16,18},{18,... | collective-permute-start | bytes 6291464 | tf_op jit(solution)/shard_map/ppermute | solution.py:587
  91.1 26.2 %collective-permute-start.11 = (bf16[256,2048]{1,0:T(8,128)(2,1)}, bf16[256,2048]{1,0:T(8,128)(2,1)S(1)}, u32[]{:S(2)}, u32[]{:S(2)}) collective-permute-start(bf16[256,2048]{1,0:T(8,128)(2,1)} %collective-permute-done.9.rest_5_), channel_id=1, source_target_pairs={{0,8},{2,10},{4,0},{6,2},{8,16},{10,18},{12,4},{14,6},{16,24},{18,... | collective-permute-start | bytes 3145736 | tf_op jit(solution)/shard_map/ppermute | solution.py:587
  91.5 26.3 %collective-permute-start.12 = (bf16[256,2048]{1,0:T(8,128)(2,1)}, bf16[256,2048]{1,0:T(8,128)(2,1)}, u32[]{:S(2)}, u32[]{:S(2)}) collective-permute-start(bf16[256,2048]{1,0:T(8,128)(2,1)} %collective-permute-done.10.rest_6_), channel_id=1, source_target_pairs={{0,4},{2,6},{4,12},{6,14},{8,0},{10,2},{12,20},{14,22},{16,8},{18,... | collective-permute-start | bytes 3145736 | tf_op jit(solution)/shard_map/ppermute | solution.py:587
  93.2 46.6 %collective-permute-start.17 = (bf16[2048,256]{1,0:T(8,128)(2,1)S(1)}, bf16[2048,256]{1,0:T(8,128)(2,1)}, u32[]{:S(2)}, u32[]{:S(2)}) collective-permute-start(bf16[2048,256]{1,0:T(8,128)(2,1)S(1)} %pad_maximum_fusion.2.rest_0_), channel_id=1, source_target_pairs={{0,8},{2,10},{4,0},{6,2},{8,16},{10,18},{12,4},{14,6},{16,24},{18,... | collective-permute-start | bytes 3145736 | tf_op jit(solution)/shard_map/ppermute | solution.py:587
  95.1 45.3 %collective-permute-start.18 = (bf16[2048,256]{1,0:T(8,128)(2,1)S(1)}, bf16[2048,256]{1,0:T(8,128)(2,1)S(1)}, u32[]{:S(2)}, u32[]{:S(2)}) collective-permute-start(bf16[2048,256]{1,0:T(8,128)(2,1)S(1)} %pad_maximum_fusion.2.rest_0_), channel_id=1, source_target_pairs={{0,4},{2,6},{4,12},{6,14},{8,0},{10,2},{12,20},{14,22},{16,8},{18,... | collective-permute-start | bytes 3145736 | tf_op jit(solution)/shard_map/ppermute | solution.py:587
  117.3 35.9 %collective-permute-start.13 = (bf16[128,2048]{1,0:T(8,128)(2,1)S(1)}, bf16[128,2048]{1,0:T(8,128)(2,1)}, u32[]{:S(2)}, u32[]{:S(2)}) collective-permute-start(bf16[128,2048]{1,0:T(8,128)(2,1)S(1)} %slice.20), channel_id=1, source_target_pairs={{0,8},{2,10},{4,0},{6,2},{8,16},{10,18},{12,4},{14,6},{16,24},{18,... | collective-permute-start | bytes 1572872 | tf_op jit(solution)/shard_map/ppermute | solution.py:587
  119.8 33.5 %collective-permute-start.14 = (bf16[128,2048]{1,0:T(8,128)(2,1)}, bf16[128,2048]{1,0:T(8,128)(2,1)}, u32[]{:S(2)}, u32[]{:S(2)}) collective-permute-start(bf16[128,2048]{1,0:T(8,128)(2,1)} %slice.21), channel_id=1, source_target_pairs={{0,4},{2,6},{4,12},{6,14},{8,0},{10,2},{12,20},{14,22},{16,8},{18,... | collective-permute-start | bytes 1572872 | tf_op jit(solution)/shard_map/ppermute | solution.py:587
  139.9 32.0 %collective-permute-start.20 = (bf16[2048,256]{1,0:T(8,128)(2,1)}, bf16[2048,256]{1,0:T(8,128)(2,1)S(1)}, u32[]{:S(2)}, u32[]{:S(2)}) collective-permute-start(bf16[2048,256]{1,0:T(8,128)(2,1)} %collective-permute-done.17.rest_0_), channel_id=1, source_target_pairs={{0,8},{2,10},{4,0},{6,2},{8,16},{10,18},{12,4},{14,6},{16,24},{18,... | collective-permute-start | bytes 3145736 | tf_op jit(solution)/shard_map/ppermute | solution.py:587
  140.4 31.5 %collective-permute-start.21 = (bf16[2048,256]{1,0:T(8,128)(2,1)S(1)}, bf16[2048,256]{1,0:T(8,128)(2,1)S(1)}, u32[]{:S(2)}, u32[]{:S(2)}) collective-permute-start(bf16[2048,256]{1,0:T(8,128)(2,1)S(1)} %collective-permute-done.18.rest_1_), channel_id=1, source_target_pairs={{0,4},{2,6},{4,12},{6,14},{8,0},{10,2},{12,20},{14,22},{16,8},{18,... | collective-permute-start | bytes 3145736 | tf_op jit(solution)/shard_map/ppermute | solution.py:587
  176.7 25.6 %collective-permute-start.24 = (bf16[2048,256]{1,0:T(8,128)(2,1)S(1)}, bf16[2048,256]{1,0:T(8,128)(2,1)S(1)}, u32[]{:S(2)}, u32[]{:S(2)}) collective-permute-start(bf16[2048,256]{1,0:T(8,128)(2,1)S(1)} %collective-permute-done.21.rest_1_), channel_id=1, source_target_pairs={{0,4},{2,6},{4,12},{6,14},{8,0},{10,2},{12,20},{14,22},{16,8},{18,... | collective-permute-start | bytes 3145736 | tf_op jit(solution)/shard_map/ppermute | solution.py:587
  178.5 25.2 %collective-permute-start.23 = (bf16[2048,256]{1,0:T(8,128)(2,1)S(1)}, bf16[2048,256]{1,0:T(8,128)(2,1)S(1)}, u32[]{:S(2)}, u32[]{:S(2)}) collective-permute-start(bf16[2048,256]{1,0:T(8,128)(2,1)S(1)} %collective-permute-done.20.rest_0_), channel_id=1, source_target_pairs={{0,8},{2,10},{4,0},{6,2},{8,16},{10,18},{12,4},{14,6},{16,24},{18,... | collective-permute-start | bytes 3145736 | tf_op jit(solution)/shard_map/ppermute | solution.py:587
  210.1 18.7 %collective-permute-start.19 = (bf16[1024,512]{1,0:T(8,128)(2,1)S(1)}, bf16[1024,512]{1,0:T(8,128)(2,1)S(1)}, u32[]{:S(2)}, u32[]{:S(2)}) collective-permute-start(bf16[1024,512]{1,0:T(8,128)(2,1)S(1)} %share_of.6), channel_id=1, source_target_pairs={{0,2},{2,0},{4,6},{6,4},{8,10},{10,8},{12,14},{14,12},{16,18},{18,... | collective-permute-start | bytes 3145736 | tf_op jit(solution)/shard_map/ppermute | solution.py:587
  214.3 20.4 %collective-permute-start.16 = (bf16[1024,256]{1,0:T(8,128)(2,1)S(1)}, bf16[1024,256]{1,0:T(8,128)(2,1)S(1)}, u32[]{:S(2)}, u32[]{:S(2)}) collective-permute-start(bf16[1024,256]{1,0:T(8,128)(2,1)S(1)} %share_of.5), channel_id=1, source_target_pairs={{0,2},{2,0},{4,6},{6,4},{8,10},{10,8},{12,14},{14,12},{16,18},{18,... | collective-permute-start | bytes 1572872 | tf_op jit(solution)/shard_map/ppermute | solution.py:587
  227.5 43.0 %collective-permute-start.31 = (bf16[512,512]{1,0:T(8,128)(2,1)S(1)}, bf16[512,512]{1,0:T(8,128)(2,1)S(1)}, u32[]{:S(2)}, u32[]{:S(2)}) collective-permute-start(bf16[512,512]{1,0:T(8,128)(2,1)S(1)} %get-tuple-element.32), channel_id=1, source_target_pairs={{0,1},{1,0},{2,3},{3,2},{4,5},{5,4},{6,7},{7,6},{8,9},{9,8},{10,11... | collective-permute-start | bytes 1572872 | tf_op jit(solution)/shard_map/ppermute | solution.py:587
  232.6 37.9 %collective-permute-start.30 = (bf16[512,512]{1,0:T(8,128)(2,1)S(1)}, bf16[512,512]{1,0:T(8,128)(2,1)S(1)}, u32[]{:S(2)}, u32[]{:S(2)}) collective-permute-start(bf16[512,512]{1,0:T(8,128)(2,1)S(1)} %get-tuple-element.41), channel_id=1, source_target_pairs={{0,1},{1,0},{2,3},{3,2},{4,5},{5,4},{6,7},{7,6},{8,9},{9,8},{10,11... | collective-permute-start | bytes 1572872 | tf_op jit(solution)/shard_map/ppermute | solution.py:587
  233.4 37.0 %collective-permute-start.32 = (bf16[512,512]{1,0:T(8,128)(2,1)S(1)}, bf16[512,512]{1,0:T(8,128)(2,1)S(1)}, u32[]{:S(2)}, u32[]{:S(2)}) collective-permute-start(bf16[512,512]{1,0:T(8,128)(2,1)S(1)} %get-tuple-element.36), channel_id=1, source_target_pairs={{0,1},{1,0},{2,3},{3,2},{4,5},{5,4},{6,7},{7,6},{8,9},{9,8},{10,11... | collective-permute-start | bytes 1572872 | tf_op jit(solution)/shard_map/ppermute | solution.py:587
  236.2 34.3 %collective-permute-start.29 = (bf16[512,256]{1,0:T(8,128)(2,1)S(1)}, bf16[512,256]{1,0:T(8,128)(2,1)S(1)}, u32[]{:S(2)}, u32[]{:S(2)}) collective-permute-start(bf16[512,256]{1,0:T(8,128)(2,1)S(1)} %get-tuple-element.40), channel_id=1, source_target_pairs={{0,1},{1,0},{2,3},{3,2},{4,5},{5,4},{6,7},{7,6},{8,9},{9,8},{10,11... | collective-permute-start | bytes 786440 | tf_op jit(solution)/shard_map/ppermute | solution.py:587
  238.4 37.1 %collective-permute-start.33 = (bf16[512,256]{1,0:T(8,128)(2,1)S(1)}, bf16[512,256]{1,0:T(8,128)(2,1)S(1)}, u32[]{:S(2)}, u32[]{:S(2)}) collective-permute-start(bf16[512,256]{1,0:T(8,128)(2,1)S(1)} %get-tuple-element.42), channel_id=1, source_target_pairs={{0,1},{1,0},{2,3},{3,2},{4,5},{5,4},{6,7},{7,6},{8,9},{9,8},{10,11... | collective-permute-start | bytes 786440 | tf_op jit(solution)/shard_map/ppermute | solution.py:587
  (32 other events, 457.4 us)
